TPU v7x, 32 devices: a whole 2x2x4 slice. The times are simulated.
32 devices in a mesh: grp: 2 (over y), sp: 4 (over z), tp: 4 (over x, core).
Axes of the slice: x: 2, y: 2, z: 4, core: 2. Of those that a mesh axis runs over, the one named last changes fastest.
Arguments:
- residual: bfloat16 [2048, 2048], P(('grp', 'sp')), parts along dimension 0, may hold values from -34 to 34
- queries: bfloat16 [2048, 1024], P(('grp', 'sp'), 'tp'), parts along dimension 0, may hold values from -400 to 400
- keys: bfloat16 [2048, 512], P(('grp', 'sp'), 'tp'), parts along dimension 0, may hold values from -8 to 8
- values: bfloat16 [2048, 512], P(('grp', 'sp'), 'tp'), parts along dimension 0, may hold values from -6 to 6
- segments: int32 [2048], P(('grp', 'sp')), parts along dimension 0, may hold values from 0 to 2, never falling along the last dimension, each value on 1 to 768 neighbouring positions
- routes: int32 [2048, 2], P(('grp', 'sp')), parts along dimension 0, may hold values from 0 to 3, all different within a row; in each aligned block of 256 rows (0 to 255, 256 to 511, ...) at most 256 rows name the same one
- route_weight: float32 [2048, 2], P(('grp', 'sp')), parts along dimension 0, may hold values from 0.3 to 3
- sinks: float32 [16], P('tp'), may hold values from 1 to 6
- out_weight: bfloat16 [1024, 2048], P('tp'), may hold values from -1 to 1
- norm_gain: float32 [2048], replicated, may hold values from 0.1 to 1.9
- expert_gate: bfloat16 [4, 2048, 1024], P('sp', None, 'tp'), may hold values from -0.125 to 0.125
- expert_up: bfloat16 [4, 2048, 1024], P('sp', None, 'tp'), may hold values from -0.125 to 0.125
- expert_down: bfloat16 [4, 1024, 2048], P('sp', None, 'tp'), may hold values from -0.1875 to 0.1875
- shared_gate: bfloat16 [2048, 1024], P(None, 'tp'), may hold values from -0.125 to 0.125
- shared_up: bfloat16 [2048, 1024], P(None, 'tp'), may hold values from -0.125 to 0.125
- shared_down: bfloat16 [1024, 2048], P(None, 'tp'), may hold values from -0.1875 to 0.1875
Outputs:
- mixed: bfloat16 [2048, 2048], P(('grp', 'sp'), 'tp'), parts along dimension 0
There are 2 independent parts, one for each index of `grp`. A program takes and returns all parts, laid end to end along the dimension named above; an argument that names none is the same for every part. Nothing has to cross between parts.
Inputs may be any that keep to these rules, and one draw needn't show every extreme that they name: `routes`: each row names 2 different experts. In the rows of one device no expert is named by more than 256 rows, and in some device's rows an expert is named by exactly 256. `segments`: document numbers never fall along the positions; every document spans 1 to 768 positions and one spans exactly 768.
All inputs are finite; a program needn't handle non-finite values.
Results may differ from a plain program's by a relative error of at most 0.0065.
Values may be sent and summed in bfloat16 or wider, within the bound.
A program may use at most 64 MiB of HBM per device.

v0:
```python
import functools
import jax
import jax.numpy as jnp
from jax import lax
from jax.experimental import pallas as pl
from jax.experimental.pallas import tpu as pltpu
from jax.sharding import PartitionSpec as P

HEAD_DIM = 64
WINDOW = 128


epsilon = 1e-06


def passed_along(value, axis, steps):
    count = lax.axis_size(axis)
    leading, last = (max(0, -steps), min(count, count - steps))
    return lax.ppermute(value, axis, [(source, source + steps) for source in range(leading, last)])


def banded(prev_rows, own_rows, window_len):
    blocks = own_rows.shape[0] // window_len
    joined = jnp.concatenate([prev_rows, own_rows], axis=0)
    shaped = joined.reshape((blocks + 1, window_len) + own_rows.shape[1:])
    return jnp.concatenate([shaped[:-1], shaped[1:]], axis=1)


def shards(
    residual,
    queries,
    keys,
    values,
    segments,
    routes,
    route_weight,
    sinks,
    out_weight,
    norm_gain,
    expert_gate,
    expert_up,
    expert_down,
    shared_gate,
    shared_up,
    shared_down,
):
    rows_here = residual.shape[0]
    model_width = residual.shape[1]
    tp_count = lax.axis_size("tp")
    tp_index = lax.axis_index("tp")
    head_local = queries.shape[1] // HEAD_DIM
    kv_local = keys.shape[1] // HEAD_DIM
    group_size = head_local // kv_local
    window_len = WINDOW
    blocks = rows_here // window_len
    own_marks = (segments % 256 + 1).astype(jnp.bfloat16)
    prev_keys, prev_values, prev_marks = passed_along(
        (
            keys[rows_here - window_len :],
            values[rows_here - window_len :],
            own_marks[rows_here - window_len :],
        ),
        "sp",
        1,
    )
    key_band = banded(prev_keys, keys, window_len).reshape(
        blocks, 2 * window_len, kv_local, HEAD_DIM
    )
    value_band = banded(prev_values, values, window_len).reshape(
        blocks, 2 * window_len, kv_local, HEAD_DIM
    )
    mark_band = banded(prev_marks, own_marks, window_len).astype(jnp.float32)
    query_marks = own_marks.reshape(blocks, window_len).astype(jnp.float32)
    query_blocks = queries.reshape(blocks, window_len, kv_local, group_size, HEAD_DIM)
    scores = jnp.einsum(
        "nqhgd,nkhd->nhgqk", query_blocks, key_band, preferred_element_type=jnp.float32
    ) * HEAD_DIM ** (-0.5)
    offsets = jnp.arange(window_len)[:, None] + window_len - jnp.arange(2 * window_len)[None, :]
    allowed = (
        (offsets >= 0) & (offsets < window_len) & (query_marks[:, :, None] == mark_band[:, None, :])
    )
    sink_logits = sinks.reshape(kv_local, group_size)[None, :, :, None]
    masked = jnp.where(allowed[:, None, None], scores, -jnp.inf)
    top_score = jnp.maximum(jnp.max(masked, axis=-1), sink_logits)
    exp_terms = jnp.where(allowed[:, None, None], jnp.exp(scores - top_score[..., None]), 0.0)
    denominator = jnp.sum(exp_terms, axis=-1) + jnp.exp(sink_logits - top_score)
    probabilities = (exp_terms / denominator[..., None]).astype(jnp.bfloat16)
    attended = jnp.einsum(
        "nhgqk,nkhd->nqhgd", probabilities, value_band, preferred_element_type=jnp.float32
    )
    attended = attended.astype(jnp.bfloat16).reshape(rows_here, head_local * HEAD_DIM)
    partial_value = jnp.dot(attended, out_weight, preferred_element_type=jnp.float32)
    col_width = model_width // tp_count
    col_start = tp_index * col_width
    summed = lax.psum(partial_value, "tp")
    updated = (residual.astype(jnp.float32) + summed).astype(jnp.bfloat16)
    updated_f32 = updated.astype(jnp.float32)
    inv_rms = lax.rsqrt(jnp.mean(updated_f32 * updated_f32, axis=-1, keepdims=True) + epsilon)
    normed = (updated_f32 * inv_rms * norm_gain).astype(jnp.bfloat16)
    updated_cols = lax.dynamic_slice_in_dim(updated, col_start, col_width, 1)
    normed_cols = lax.dynamic_slice_in_dim(normed, col_start, col_width, 1)
    shared_pre = jnp.dot(normed, shared_gate, preferred_element_type=jnp.float32)
    shared_lin = jnp.dot(normed, shared_up, preferred_element_type=jnp.float32)
    shared_act = (jax.nn.silu(shared_pre) * shared_lin).astype(jnp.bfloat16)
    top_count = routes.shape[1]
    experts = lax.axis_size("sp")
    capacity = 2 * rows_here * top_count // experts
    flat_ids = routes.reshape(-1)
    one_hot = (flat_ids[:, None] == jnp.arange(experts, dtype=jnp.int32)[None, :]).astype(jnp.int32)
    rank_in = jnp.cumsum(one_hot, axis=0) - one_hot
    slot_dest = flat_ids * capacity + jnp.sum(rank_in * one_hot, axis=1)
    token_of = jnp.arange(rows_here * top_count, dtype=jnp.int32) // top_count
    slot_token = jnp.full((experts * capacity,), -1, jnp.int32).at[slot_dest].set(token_of)
    filled = slot_token >= 0
    safe_token = jnp.where(filled, slot_token, 0)
    outgoing = jnp.where(filled[:, None], normed_cols[safe_token], jnp.zeros((), jnp.bfloat16))
    pieces = lax.all_to_all(
        outgoing.reshape(experts, capacity, col_width),
        "sp",
        split_axis=0,
        concat_axis=0,
        tiled=True,
    )
    arrived = lax.all_gather(pieces, "tp", axis=2, tiled=True)
    expert_rows = arrived.reshape(-1, model_width)
    gate_pre = jnp.dot(expert_rows, expert_gate[0], preferred_element_type=jnp.float32)
    up_lin = jnp.dot(expert_rows, expert_up[0], preferred_element_type=jnp.float32)
    expert_act = (jax.nn.silu(gate_pre) * up_lin).astype(jnp.bfloat16)
    gathered_expert, gathered_shared = (
        lax.all_gather(expert_act, "tp", axis=1, tiled=True),
        lax.all_gather(shared_act, "tp", axis=1, tiled=True),
    )
    expert_out = jnp.dot(
        gathered_expert, expert_down[0], preferred_element_type=jnp.float32
    ).astype(jnp.bfloat16)
    returned = lax.all_to_all(
        expert_out.reshape(experts, capacity, col_width),
        "sp",
        split_axis=0,
        concat_axis=0,
        tiled=True,
    )
    returned = returned.reshape(experts * capacity, col_width)
    picked = returned[slot_dest].astype(jnp.float32).reshape(rows_here, top_count, col_width)
    routed = jnp.sum(picked * route_weight[:, :, None], axis=1)
    shared_cols = jnp.dot(gathered_shared, shared_down, preferred_element_type=jnp.float32)
    return (updated_cols.astype(jnp.float32) + shared_cols + routed).astype(jnp.bfloat16)


MESH = pl.DeviceIdType.MESH
PARTS = 4
ALONG = 1


def fused_kernel(
    dims,
    res_hbm,
    q_ref,
    k_ref,
    v_ref,
    seg_ref,
    routes_ref,
    rw_ref,
    sinks_ref,
    wo_hbm,
    gain_ref,
    eg_hbm,
    eu_hbm,
    ed_hbm,
    sg_hbm,
    su_hbm,
    sd_hbm,
    out_ref,
    res_v,
    wo_v,
    gu_v,
    sgu_v,
    dn_v,
    sdn_v,
    kh,
    vh,
    mh,
    marks_v,
    aux_rows,
    aux_ref,
    att,
    b1s,
    b1r,
    b2s,
    b2r,
    keep,
    upd,
    norm_v,
    act,
    eout,
    eback,
    acc,
    w_sem,
    halo_s,
    halo_r,
    b_s,
    b_r,
    u_s,
    u_r,
    a_s,
    a_r,
    e_s,
    e_r,
):
    rows, cols, width, window, hidden, heads, group = dims
    bf16, f32 = jnp.bfloat16, jnp.float32
    s = lax.axis_index("sp")
    t = lax.axis_index("tp")
    core = t % 2
    chip = t // 2
    mate = t + 1 - 2 * core
    over = t + 2 - 4 * chip
    diag = 3 - t

    def remote(src, dst, send, recv, sp, tp):
        return pltpu.make_async_remote_copy(
            src_ref=src,
            dst_ref=dst,
            send_sem=send,
            recv_sem=recv,
            device_id={"sp": sp, "tp": tp},
            device_id_type=MESH,
        )

    barrier = pltpu.get_barrier_semaphore()
    pl.semaphore_signal(barrier, inc=1, device_id={"sp": s, "tp": mate}, device_id_type=MESH)
    pl.semaphore_signal(barrier, inc=1, device_id={"sp": s, "tp": over}, device_id_type=MESH)
    for step in range(1, 4):
        pl.semaphore_signal(
            barrier, inc=1, device_id={"sp": (s + step) % 4, "tp": t}, device_id_type=MESH
        )

    own_cols = pl.ds(pl.multiple_of(t * cols, cols), cols)
    loads = [
        pltpu.make_async_copy(wo_hbm, wo_v, w_sem.at[0]),
        pltpu.make_async_copy(res_hbm.at[:, own_cols], res_v, w_sem.at[1]),
        pltpu.make_async_copy(eg_hbm.at[0], gu_v.at[:, pl.ds(0, hidden)], w_sem.at[2]),
        pltpu.make_async_copy(eu_hbm.at[0], gu_v.at[:, pl.ds(hidden, hidden)], w_sem.at[3]),
        pltpu.make_async_copy(sg_hbm, sgu_v.at[:, pl.ds(0, hidden)], w_sem.at[4]),
        pltpu.make_async_copy(su_hbm, sgu_v.at[:, pl.ds(hidden, hidden)], w_sem.at[5]),
        pltpu.make_async_copy(ed_hbm.at[0], dn_v, w_sem.at[6]),
        pltpu.make_async_copy(sd_hbm, sdn_v, w_sem.at[7]),
    ]
    for load in loads[:2]:
        load.start()

    top_count = routes_ref.shape[0]
    aux_rows[...] = jnp.zeros_like(aux_rows)
    aux_rows[0:1, :] = seg_ref[...].astype(f32)
    aux_rows[1 : 1 + top_count, :] = routes_ref[...].astype(f32)
    aux_rows[1 + top_count : 1 + 2 * top_count, :] = rw_ref[...]
    marks_v[...] = jnp.broadcast_to(aux_rows[0:1, pl.ds(rows - window, window)], (8, window))
    def marks_across(n):
        return aux_rows[0:1, pl.ds(n * window, window)]

    tail = pl.ds(rows - window, window)
    up_sp, down_sp = (s + 1) % 4, (s + 3) % 4
    halos = [
        remote(k_ref.at[tail], kh, halo_s.at[0], halo_r.at[0], up_sp, t),
        remote(v_ref.at[tail], vh, halo_s.at[1], halo_r.at[1], up_sp, t),
        remote(marks_v, mh, halo_s.at[2], halo_r.at[2], up_sp, t),
    ]

    @pl.when(s == 0)
    def _():
        kh[...] = jnp.zeros_like(kh)
        vh[...] = jnp.zeros_like(vh)
        mh[...] = jnp.full(mh.shape, -1.0, f32)

    for n in range(rows // window):
        here = pl.ds(n * window, window)
        aux_ref[here, :] = jnp.transpose(aux_rows[:, here])

    q_pos = lax.broadcasted_iota(jnp.int32, (window, window), 0)
    k_pos = lax.broadcasted_iota(jnp.int32, (window, window), 1)

    def attend(n):
        here = pl.ds(n * window, window)
        if n == 0:
            k_prev, v_prev, m_prev = kh[...], vh[...], mh[0:1, :]
        else:
            before = pl.ds((n - 1) * window, window)
            k_prev, v_prev, m_prev = k_ref[before, :], v_ref[before, :], marks_across(n - 1)
        k_own, v_own, m_own = k_ref[here, :], v_ref[here, :], marks_across(n)
        marks = aux_ref[here, 0:1]
        ok_prev = (k_pos > q_pos) & (marks == m_prev)
        ok_own = (k_pos <= q_pos) & (marks == m_own)
        for h in range(heads):
            kv = slice((h // group) * HEAD_DIM, (h // group + 1) * HEAD_DIM)
            qh = q_ref[here, h * HEAD_DIM : (h + 1) * HEAD_DIM]
            contract = (((1,), (1,)), ((), ()))
            sc_prev = lax.dot_general(
                qh, k_prev[:, kv], contract, preferred_element_type=f32
            ) * HEAD_DIM ** (-0.5)
            sc_own = lax.dot_general(
                qh, k_own[:, kv], contract, preferred_element_type=f32
            ) * HEAD_DIM ** (-0.5)
            sc_prev = jnp.where(ok_prev, sc_prev, -jnp.inf)
            sc_own = jnp.where(ok_own, sc_own, -jnp.inf)
            sink = sinks_ref[h]
            top = jnp.maximum(
                jnp.max(jnp.maximum(sc_prev, sc_own), axis=-1, keepdims=True), sink
            )
            ex_prev = jnp.exp(sc_prev - top)
            ex_own = jnp.exp(sc_own - top)
            total = jnp.sum(ex_prev + ex_own, axis=-1, keepdims=True) + jnp.exp(sink - top)
            inverse = 1.0 / total
            p_prev = (ex_prev * inverse).astype(bf16)
            p_own = (ex_own * inverse).astype(bf16)
            got = jnp.dot(p_prev, v_prev[:, kv], preferred_element_type=f32) + jnp.dot(
                p_own, v_own[:, kv], preferred_element_type=f32
            )
            att[here, h * HEAD_DIM : (h + 1) * HEAD_DIM] = got.astype(bf16)

    def project(n, chunk):
        where = pl.ds(pl.multiple_of(chunk * cols, cols), cols)
        return jnp.dot(
            att[pl.ds(n * window, window), :], wo_v[:, where], preferred_element_type=f32
        )

    halves = list(range(rows // window))[::-1]
    attend(halves[0])
    pl.semaphore_wait(barrier, 5)

    @pl.when(s < 3)
    def _():
        for copy in halos:
            copy.start()

    pending = []
    first = {}
    second = {}
    for n in halves:
        if n == 0:

            @pl.when(s > 0)
            def _():
                for copy in halos:
                    copy.wait_recv()

        if n != halves[0]:
            attend(n)
        else:
            loads[0].wait()
            for load in loads[2:]:
                load.start()
        for far in (1, 0):
            chunk = (over if far else t) + 1 - 2 * core
            b1s[n, far] = project(n, chunk).astype(bf16)
            copy = remote(
                b1s.at[n, far], b1r.at[n, far], b_s.at[n, far], b_r.at[n, far], s, mate
            )
            copy.start()
            pending.append(copy)
            first[n, far] = copy
        mine = project(n, over)
        first[n, 1].wait_recv()
        b2s[n] = (mine + b1r[n, 1].astype(f32)).astype(bf16)
        copy = remote(b2s.at[n], b2r.at[n], b_s.at[n, 2], b_r.at[n, 2], s, over)
        copy.start()
        pending.append(copy)
        second[n] = copy
    loads[1].wait()
    for n in halves:
        here = pl.ds(n * window, window)
        mine = project(n, t) + res_v[here, :].astype(f32)
        first[n, 0].wait_recv()
        keep[here, :] = mine + b1r[n, 0].astype(f32)

    parts = u_s.shape[2]
    part_rows = rows // parts
    per_half = window // part_rows
    listed = [n * per_half + i for n in halves for i in range(per_half)]

    def of_half(n):
        return [p for p in listed if n is None or p // per_half == n]

    def piece(b, chunk, n):
        return upd.at[b, chunk, pl.ds(n * part_rows, part_rows)]

    def share(kind, k, b, chunk, n, sp, tp):
        return remote(
            piece(b, chunk, n),
            piece(b, chunk, n),
            u_s.at[kind, k, n],
            u_r.at[b, chunk, n],
            sp,
            tp,
        )

    conditional = []
    for n in halves:
        here = pl.ds(n * window, window)
        second[n].wait_recv()
        upd[s, t, here, :] = (keep[here, :] + b2r[n].astype(f32)).astype(bf16)
        for p in of_half(n):
            over_copy = share(3, 0, s, t, p, s, over)
            over_copy.start()
            up_copy = share(0, 0, s, t, p, up_sp, t)
            down_copy = share(1, 0, s, t, p, down_sp, t)

            @pl.when(s < 3)
            def _(up_copy=up_copy):
                up_copy.start()

            @pl.when(s > 0)
            def _(down_copy=down_copy):
                down_copy.start()

            mate_copy = share(2, 0, s, t, p, s, mate)
            mate_copy.start()
            pending += [over_copy, mate_copy]
            conditional += [(s < 3, up_copy), (s > 0, down_copy)]

    side = s // 2
    edge = s + side * (3 - 2 * s)
    order = [s]
    for k in range(1, 4):
        flat = (k, k + edge, k - 2 * edge, k)[k]
        order.append(flat + side * (3 - 2 * flat))

    along = listed[:ALONG]

    def onward(k, kinds, chunk, n):
        b = order[k]
        to_up = share(kinds[0], k, b, chunk, n, up_sp, t)
        to_down = share(kinds[1], k, b, chunk, n, down_sp, t)
        rising = s < 3 if k == 0 else (b < s) & (s < 3)
        falling = s > 0 if k == 0 else (b > s) & (s > 0)

        @pl.when(rising)
        def _():
            to_up.start()

        @pl.when(falling)
        def _():
            to_down.start()

        conditional.extend([(rising, to_up), (falling, to_down)])

    def arrive(k, half=None):
        b = order[k]
        for n in of_half(half):
            share(0, k, b, t, n, s, mate).wait_recv()
            onward(k, (0, 1), t, n)
            if n not in along:
                copy = share(3, k, b, t, n, s, over)
                copy.start()
                pending.append(copy)
            mate_copy = share(2, k, b, t, n, s, mate)
            mate_copy.start()
            pending.append(mate_copy)

    def relay_half(k, n):
        b = order[k]
        share(4, k, b, over, n, s, mate).wait_recv()
        if n in along:
            onward(k, (5, 6), over, n)
        copy = share(4, k, b, over, n, s, mate)
        copy.start()
        pending.append(copy)

    def relay(k, half=None):
        for n in of_half(half):
            if k == 0 or n not in along:
                relay_half(k, n)

    def arrive_over(k):
        for n in along:
            relay_half(k, n)

    def span_of(half):
        if half is None:
            return halves, 0, rows
        return [half], half * window, window

    def normalize(k, half=None):
        b = order[k]
        _, begin, length = span_of(half)
        for n in of_half(half):
            share(2, k, b, mate, n, s, mate).wait_recv()
            share(4, k, b, diag, n, s, mate).wait_recv()
        step = 32

        def body(i, carry):
            here = pl.ds(pl.multiple_of(begin + i * step, step), step)
            squares = jnp.zeros((step, 1), f32)
            for chunk in range(4):
                part = upd[b, chunk, here, :].astype(f32)
                squares = squares + jnp.sum(part * part, axis=-1, keepdims=True)
            inv = lax.rsqrt(squares / width + epsilon)
            for chunk in range(4):
                part = upd[b, chunk, here, :].astype(f32)
                span = slice(chunk * cols, (chunk + 1) * cols)
                norm_v[here, span] = (part * inv * gain_ref[0:1, span]).astype(bf16)
            return carry

        lax.fori_loop(0, length // step, body, 0)

    def pass_on(slot, kind, chunk, tp, half):
        place = act.at[slot, chunk, pl.ds(half * window, window)]
        return remote(
            place, place, a_s.at[kind, slot, half], a_r.at[slot, chunk, half], s, tp
        )

    def activate(slot, weight, half=None):
        _, begin, length = span_of(half)
        here = pl.ds(begin, length)
        both = jnp.dot(norm_v[here, :], weight[...], preferred_element_type=f32)
        gate, lin = both[:, :hidden], both[:, hidden:]
        act[slot, t, here, :] = (gate / (1.0 + jnp.exp(-gate)) * lin).astype(bf16)

    def ship(slot, half=None):
        for n in span_of(half)[0]:
            for kind, tp in ((0, over), (1, mate)):
                copy = pass_on(slot, kind, t, tp, n)
                copy.start()
                pending.append(copy)

    def relay_act(slot, half=None):
        for n in span_of(half)[0]:
            pass_on(slot, 2, over, mate, n).wait_recv()
            copy = pass_on(slot, 2, over, mate, n)
            copy.start()
            pending.append(copy)

    def contract_act(slot, weight, half=None):
        listing, begin, length = span_of(half)
        for n in listing:
            pass_on(slot, 1, mate, mate, n).wait_recv()
            pass_on(slot, 2, diag, mate, n).wait_recv()
        total = None
        for chunk in range(4):
            part = jnp.dot(
                act[slot, chunk, pl.ds(begin, length), :],
                weight[chunk * hidden : (chunk + 1) * hidden, :],
                preferred_element_type=f32,
            )
            total = part if total is None else total + part
        return total

    def give_back(k, b, half):
        here = pl.ds(half * window, window)
        return remote(
            eout.at[k, here], eback.at[b, here], e_s.at[k, half], e_r.at[b, half], order[k], t
        )

    def finish(k, half=None):
        listing, begin, length = span_of(half)
        eout[k, pl.ds(begin, length), :] = contract_act(k, dn_v, half).astype(bf16)
        for n in listing:
            copy = give_back(k, s, n)
            copy.start()
            pending.append(copy)

    def expert(k, half=None):
        normalize(k, half)
        activate(k, gu_v, half)
        ship(k, half)

    early, late = halves[0], halves[-1]
    arrive(1)
    relay(0)
    arrive(2)
    arrive_over(1)
    relay(1)
    loads[2].wait()
    loads[3].wait()
    expert(1)
    arrive(3, early)
    arrive_over(2)
    normalize(0)
    activate(0, gu_v)
    relay(2)
    loads[4].wait()
    loads[5].wait()
    activate(4, sgu_v)
    expert(2)
    relay_act(1)
    loads[6].wait()
    finish(1)
    arrive(3, late)
    arrive_over(3)
    relay(3, early)
    expert(3, early)
    relay_act(2)
    finish(2)
    relay(3, late)
    expert(3, late)
    ship(0)
    ship(4)
    relay_act(3, early)
    finish(3, early)
    relay_act(3, late)
    finish(3, late)
    relay_act(0)
    relay_act(4)
    eout[0] = contract_act(0, dn_v).astype(bf16)
    loads[7].wait()
    acc[...] = contract_act(4, sdn_v)

    def weight_of(e):
        total = jnp.zeros((rows, 1), f32)
        for k in range(1, top_count + 1):
            weight = aux_ref[:, top_count + k : top_count + k + 1]
            named = aux_ref[:, k : k + 1] == jnp.full((rows, 1), e, jnp.int32).astype(f32)
            total = total + jnp.where(named, weight, 0.0)
        return total

    weights = [weight_of(order[k]) for k in range(4)]
    for n in halves:
        here = pl.ds(n * window, window)
        acc[here, :] = (
            acc[here, :]
            + upd[s, t, here, :].astype(f32)
            + weights[0][n * window : (n + 1) * window] * eout[0, here, :].astype(f32)
        )
    for k in range(1, 4):
        for n in halves:
            here = pl.ds(n * window, window)
            give_back(k, order[k], n).wait_recv()
            more = weights[k][n * window : (n + 1) * window] * eback[order[k], here, :].astype(f32)
            if k < 3:
                acc[here, :] = acc[here, :] + more
            else:
                out_ref[here, :] = (acc[here, :] + more).astype(bf16)

    for copy in pending:
        copy.wait_send()
    for when, copy in conditional:

        @pl.when(when)
        def _():
            copy.wait_send()

    @pl.when(s < 3)
    def _():
        for copy in halos:
            copy.wait_send()


def layer(
    residual,
    queries,
    keys,
    values,
    segments,
    routes,
    route_weight,
    sinks,
    out_weight,
    norm_gain,
    expert_gate,
    expert_up,
    expert_down,
    shared_gate,
    shared_up,
    shared_down,
):
    arguments = (
        residual,
        queries,
        keys,
        values,
        segments,
        routes,
        route_weight,
        sinks,
        out_weight,
        norm_gain,
        expert_gate,
        expert_up,
        expert_down,
        shared_gate,
        shared_up,
        shared_down,
    )
    rows, width = residual.shape
    n_sp, n_tp = lax.axis_size("sp"), lax.axis_size("tp")
    capacity = 2 * rows * routes.shape[1] // n_sp
    hidden = expert_gate.shape[2]
    if n_sp != 4 or n_tp != 4 or capacity < rows or rows < 2 * WINDOW or shared_gate.shape[1] != hidden:
        return shards(*arguments)
    cols = width // n_tp
    heads = queries.shape[1] // HEAD_DIM
    group = queries.shape[1] // keys.shape[1]
    kv_width = keys.shape[1]
    blocks = rows // WINDOW
    bf16, f32 = jnp.bfloat16, jnp.float32
    vmem = pl.BlockSpec(memory_space=pltpu.VMEM)
    anywhere = pl.BlockSpec(memory_space=pl.ANY)
    dma = pltpu.SemaphoreType.DMA
    return pl.pallas_call(
        functools.partial(fused_kernel, (rows, cols, width, WINDOW, hidden, heads, group)),
        out_shape=jax.ShapeDtypeStruct((rows, cols), bf16),
        in_specs=[anywhere]
        + [vmem] * 6
        + [pl.BlockSpec(memory_space=pltpu.SMEM), anywhere, vmem]
        + [anywhere] * 6,
        out_specs=vmem,
        scratch_shapes=[
            pltpu.VMEM((rows, cols), bf16),
            pltpu.VMEM(out_weight.shape, bf16),
            pltpu.VMEM((width, 2 * hidden), bf16),
            pltpu.VMEM((width, 2 * hidden), bf16),
            pltpu.VMEM(expert_down.shape[1:], bf16),
            pltpu.VMEM(shared_down.shape, bf16),
            pltpu.VMEM((WINDOW, kv_width), bf16),
            pltpu.VMEM((WINDOW, kv_width), bf16),
            pltpu.VMEM((8, WINDOW), f32),
            pltpu.VMEM((8, WINDOW), f32),
            pltpu.VMEM((WINDOW, rows), f32),
            pltpu.VMEM((rows, WINDOW), f32),
            pltpu.VMEM((rows, heads * HEAD_DIM), bf16),
            pltpu.VMEM((blocks, 2, WINDOW, cols), bf16),
            pltpu.VMEM((blocks, 2, WINDOW, cols), bf16),
            pltpu.VMEM((blocks, WINDOW, cols), bf16),
            pltpu.VMEM((blocks, WINDOW, cols), bf16),
            pltpu.VMEM((rows, cols), f32),
            pltpu.VMEM((4, 4, rows, cols), bf16),
            pltpu.VMEM((rows, width), bf16),
            pltpu.VMEM((5, 4, rows, hidden), bf16),
            pltpu.VMEM((4, rows, cols), bf16),
            pltpu.VMEM((4, rows, cols), bf16),
            pltpu.VMEM((rows, cols), f32),
            dma((8,)),
            dma((3,)),
            dma((3,)),
            dma((blocks, 3)),
            dma((blocks, 3)),
            dma((7, 4, PARTS)),
            dma((4, 4, PARTS)),
            dma((3, 5, blocks)),
            dma((5, 4, blocks)),
            dma((4, blocks)),
            dma((4, blocks)),
        ],
        compiler_params=pltpu.CompilerParams(collective_id=0, has_side_effects=True),
    )(
        residual,
        queries,
        keys,
        values,
        segments[None, :],
        routes.T,
        route_weight.T,
        sinks,
        out_weight,
        norm_gain[None, :],
        expert_gate,
        expert_up,
        expert_down,
        shared_gate,
        shared_up,
        shared_down,
    )


def solution(mesh):
    placed = (
        P(("grp", "sp"), None),
        P(("grp", "sp"), "tp"),
        P(("grp", "sp"), "tp"),
        P(("grp", "sp"), "tp"),
        P(("grp", "sp")),
        P(("grp", "sp"), None),
        P(("grp", "sp"), None),
        P("tp"),
        P("tp", None),
        P(),
        P("sp", None, "tp"),
        P("sp", None, "tp"),
        P("sp", None, "tp"),
        P(None, "tp"),
        P(None, "tp"),
        P(None, "tp"),
    )
    return jax.shard_map(
        layer, mesh=mesh, in_specs=placed, out_specs=P(("grp", "sp"), "tp"), check_vma=False
    )
```

profile of v0, /device:TPU:0, one launch (start us, length us, event | category | flops | bytes accessed | tf_op | source)
XLA Modules:
  0.0 70.0 jit_solution(4378839192913054670)
XLA Ops:
  0.0 68.3 %shard_map.154 = bf16[256,512]{1,0:T(8,128)(2,1)} custom-call(bf16[256,2048]{1,0:T(8,128)(2,1)} %res_hbm.1, bf16[256,256]{1,0:T(8,128)(2,1)} %q_ref.1, bf16[256,128]{1,0:T(8,128)(2,1)} %k_ref.1, bf16[256,128]{1,0:T(8,128)(2,1)} %v_ref.1, s32[1,256]{1,0:T(1,128)} %bitcast.7, s32[2,256]{1,0:T(2,128)} %bitcast.5, f32[2,256]{1,0:T(2,128)} %bitcast.6, ...), custom_call_target="tpu_custom_call" | custom-call | tf_op jit(solution)/shard_map/pallas_call | solution.py:698
  68.3 1.7 %copy.18 = bf16[256,512]{1,0:T(8,128)(2,1)} copy(bf16[256,512]{1,0:T(8,128)(2,1)} %shard_map.154) | data formatting | bytes 524288
where the time goes:
time: 70.1 us; the launch traced here: 70 us
  Pallas kernels  68.3 us (97%)
  local copies, waits for them, and re-layouts  1.67 us (2%)
    pallas_call x1, Pallas kernels, layer(): pl.pallas_call(functools.partial(fused_kernel, (rows, cols, width, WINDOW...  68.3 us
    unnamed x1, local copies, waits for them, and re-layouts  1.67 us

commit v1 on v0

v1 whole, which is shorter than its diff:
```python
import functools
import jax
import jax.numpy as jnp
from jax import lax
from jax.experimental import pallas as pl
from jax.experimental.pallas import tpu as pltpu
from jax.sharding import PartitionSpec as P

HEAD_DIM = 64
WINDOW = 128


epsilon = 1e-06


def passed_along(value, axis, steps):
    count = lax.axis_size(axis)
    leading, last = (max(0, -steps), min(count, count - steps))
    return lax.ppermute(value, axis, [(source, source + steps) for source in range(leading, last)])


def banded(prev_rows, own_rows, window_len):
    blocks = own_rows.shape[0] // window_len
    joined = jnp.concatenate([prev_rows, own_rows], axis=0)
    shaped = joined.reshape((blocks + 1, window_len) + own_rows.shape[1:])
    return jnp.concatenate([shaped[:-1], shaped[1:]], axis=1)


def shards(
    residual,
    queries,
    keys,
    values,
    segments,
    routes,
    route_weight,
    sinks,
    out_weight,
    norm_gain,
    expert_gate,
    expert_up,
    expert_down,
    shared_gate,
    shared_up,
    shared_down,
):
    rows_here = residual.shape[0]
    model_width = residual.shape[1]
    tp_count = lax.axis_size("tp")
    tp_index = lax.axis_index("tp")
    head_local = queries.shape[1] // HEAD_DIM
    kv_local = keys.shape[1] // HEAD_DIM
    group_size = head_local // kv_local
    window_len = WINDOW
    blocks = rows_here // window_len
    own_marks = (segments % 256 + 1).astype(jnp.bfloat16)
    prev_keys, prev_values, prev_marks = passed_along(
        (
            keys[rows_here - window_len :],
            values[rows_here - window_len :],
            own_marks[rows_here - window_len :],
        ),
        "sp",
        1,
    )
    key_band = banded(prev_keys, keys, window_len).reshape(
        blocks, 2 * window_len, kv_local, HEAD_DIM
    )
    value_band = banded(prev_values, values, window_len).reshape(
        blocks, 2 * window_len, kv_local, HEAD_DIM
    )
    mark_band = banded(prev_marks, own_marks, window_len).astype(jnp.float32)
    query_marks = own_marks.reshape(blocks, window_len).astype(jnp.float32)
    query_blocks = queries.reshape(blocks, window_len, kv_local, group_size, HEAD_DIM)
    scores = jnp.einsum(
        "nqhgd,nkhd->nhgqk", query_blocks, key_band, preferred_element_type=jnp.float32
    ) * HEAD_DIM ** (-0.5)
    offsets = jnp.arange(window_len)[:, None] + window_len - jnp.arange(2 * window_len)[None, :]
    allowed = (
        (offsets >= 0) & (offsets < window_len) & (query_marks[:, :, None] == mark_band[:, None, :])
    )
    sink_logits = sinks.reshape(kv_local, group_size)[None, :, :, None]
    masked = jnp.where(allowed[:, None, None], scores, -jnp.inf)
    top_score = jnp.maximum(jnp.max(masked, axis=-1), sink_logits)
    exp_terms = jnp.where(allowed[:, None, None], jnp.exp(scores - top_score[..., None]), 0.0)
    denominator = jnp.sum(exp_terms, axis=-1) + jnp.exp(sink_logits - top_score)
    probabilities = (exp_terms / denominator[..., None]).astype(jnp.bfloat16)
    attended = jnp.einsum(
        "nhgqk,nkhd->nqhgd", probabilities, value_band, preferred_element_type=jnp.float32
    )
    attended = attended.astype(jnp.bfloat16).reshape(rows_here, head_local * HEAD_DIM)
    partial_value = jnp.dot(attended, out_weight, preferred_element_type=jnp.float32)
    col_width = model_width // tp_count
    col_start = tp_index * col_width
    summed = lax.psum(partial_value, "tp")
    updated = (residual.astype(jnp.float32) + summed).astype(jnp.bfloat16)
    updated_f32 = updated.astype(jnp.float32)
    inv_rms = lax.rsqrt(jnp.mean(updated_f32 * updated_f32, axis=-1, keepdims=True) + epsilon)
    normed = (updated_f32 * inv_rms * norm_gain).astype(jnp.bfloat16)
    updated_cols = lax.dynamic_slice_in_dim(updated, col_start, col_width, 1)
    normed_cols = lax.dynamic_slice_in_dim(normed, col_start, col_width, 1)
    shared_pre = jnp.dot(normed, shared_gate, preferred_element_type=jnp.float32)
    shared_lin = jnp.dot(normed, shared_up, preferred_element_type=jnp.float32)
    shared_act = (jax.nn.silu(shared_pre) * shared_lin).astype(jnp.bfloat16)
    top_count = routes.shape[1]
    experts = lax.axis_size("sp")
    capacity = 2 * rows_here * top_count // experts
    flat_ids = routes.reshape(-1)
    one_hot = (flat_ids[:, None] == jnp.arange(experts, dtype=jnp.int32)[None, :]).astype(jnp.int32)
    rank_in = jnp.cumsum(one_hot, axis=0) - one_hot
    slot_dest = flat_ids * capacity + jnp.sum(rank_in * one_hot, axis=1)
    token_of = jnp.arange(rows_here * top_count, dtype=jnp.int32) // top_count
    slot_token = jnp.full((experts * capacity,), -1, jnp.int32).at[slot_dest].set(token_of)
    filled = slot_token >= 0
    safe_token = jnp.where(filled, slot_token, 0)
    outgoing = jnp.where(filled[:, None], normed_cols[safe_token], jnp.zeros((), jnp.bfloat16))
    pieces = lax.all_to_all(
        outgoing.reshape(experts, capacity, col_width),
        "sp",
        split_axis=0,
        concat_axis=0,
        tiled=True,
    )
    arrived = lax.all_gather(pieces, "tp", axis=2, tiled=True)
    expert_rows = arrived.reshape(-1, model_width)
    gate_pre = jnp.dot(expert_rows, expert_gate[0], preferred_element_type=jnp.float32)
    up_lin = jnp.dot(expert_rows, expert_up[0], preferred_element_type=jnp.float32)
    expert_act = (jax.nn.silu(gate_pre) * up_lin).astype(jnp.bfloat16)
    gathered_expert, gathered_shared = (
        lax.all_gather(expert_act, "tp", axis=1, tiled=True),
        lax.all_gather(shared_act, "tp", axis=1, tiled=True),
    )
    expert_out = jnp.dot(
        gathered_expert, expert_down[0], preferred_element_type=jnp.float32
    ).astype(jnp.bfloat16)
    returned = lax.all_to_all(
        expert_out.reshape(experts, capacity, col_width),
        "sp",
        split_axis=0,
        concat_axis=0,
        tiled=True,
    )
    returned = returned.reshape(experts * capacity, col_width)
    picked = returned[slot_dest].astype(jnp.float32).reshape(rows_here, top_count, col_width)
    routed = jnp.sum(picked * route_weight[:, :, None], axis=1)
    shared_cols = jnp.dot(gathered_shared, shared_down, preferred_element_type=jnp.float32)
    return (updated_cols.astype(jnp.float32) + shared_cols + routed).astype(jnp.bfloat16)


MESH = pl.DeviceIdType.MESH
PARTS = 4
ALONG = (0, 2)
OWN = (0, 1)
STEPS = (
    ("attend", 1),
    ("loaded", "res"),
    ("enter",),
    ("chip", 1),
    ("across", 1),
    ("hold", 1),
    ("halo",),
    ("attend", 0),
    ("publish", 2),
    ("send", "e", 0, 2, 0),
    ("weights", "m", 0),
    ("send", "m", 1, 2, 0),
    ("chip", 0),
    ("across", 0),
    ("rest",),
    ("publish", 3),
    ("weights", "m", 2),
    ("send", "m", 1, 3, 0),
    ("send", "m", 0, 3, 0),
    ("take", "m", 0, 2, 0),
    ("send", "e", 0, 3, 0),
    ("hold", 0),
    ("own_over", 2),
    ("send", "e", 0, 2, 1),
    ("send", "m", 1, 2, 1),
    ("take", "m", 0, 3, 0),
    ("loaded", "gain", "eg", "eu", "sg", "su", "ed", "sd"),
    ("publish", 0),
    ("send", "m", 0, 0, 0),
    ("take", "m", 2, 3, 0),
    ("send", "e", 0, 0, 0),
    ("publish", 1),
    ("send", "e", 0, 1, 0),
    ("weights", "e", 3),
    ("weights", "m", 3),
    ("send", "m", 0, 1, 0),
    ("take", "e", 2, 3, 0),
    ("take", "m", 0, 2, 1),
    ("send", "m", 1, 1, 0),
    ("take", "m", 3, 3, 0),
    ("take", "e", 1, 3, 0),
    ("take", "m", 0, 1, 0),
    ("take", "m", 0, 0, 0),
    ("take", "m", 0, 3, 1),
    ("own_over", 3),
    ("take", "m", 3, 2, 0),
    ("own_over", 0),
    ("send", "e", 0, 0, 1),
    ("take", "e", 3, 3, 0),
    ("take", "m", 2, 1, 0),
    ("take", "m", 3, 2, 1),
    ("take", "e", 1, 2, 1),
    ("compute_own", 1),
    ("take", "e", 1, 3, 1),
    ("own_over", 1),
    ("take", "e", 3, 2, 0),
    ("take", "e", 1, 2, 0),
    ("take", "m", 3, 1, 0),
    ("take", "m", 2, 0, 0),
    ("take", "m", 0, 0, 1),
    ("take", "m", 3, 3, 1),
    ("take", "e", 2, 1, 0),
    ("take", "e", 3, 1, 0),
    ("take", "e", 3, 3, 1),
    ("compute_own", 0),
    ("take", "m", 2, 3, 1),
    ("take", "e", 3, 2, 1),
    ("weights", "e", 2),
    ("send", "m", 0, 0, 1),
    ("take", "m", 3, 0, 0),
    ("send", "m", 0, 2, 0),
    ("compute", (3, 0), 1),
    ("take", "m", 3, 0, 1),
    ("take", "e", 2, 3, 1),
    ("take", "e", 3, 0, 0),
    ("relay", "b", 0, 1),
    ("send", "m", 0, 2, 1),
    ("take", "m", 2, 1, 1),
    ("take", "m", 2, 0, 1),
    ("weights", "e", 1),
    ("relay", "b", 1, 1),
    ("take", "m", 2, 2, 0),
    ("take", "m", 2, 2, 1),
    ("take", "e", 3, 1, 1),
    ("send", "m", 1, 0, 1),
    ("take", "e", 3, 0, 1),
    ("compute", (1, 3), 1),
    ("take", "e", 2, 0, 0),
    ("take", "e", 2, 0, 1),
    ("send", "m", 1, 0, 0),
    ("take", "e", 2, 1, 1),
    ("take", "m", 3, 1, 1),
    ("compute", (3, 3), 0),
    ("take", "e", 1, 1, 0),
    ("shared", 1),
    ("relay", "m", 3, 1),
    ("take", "m", 0, 1, 1),
    ("relay", "e", 3, 1),
    ("take", "e", 2, 2, 0),
    ("compute", (2, 2), 0),
    ("give", (3, 3), 1),
    ("own", 1),
    ("take", "e", 2, 2, 1),
    ("relay", "e", 3, 0),
    ("relay", "m", 0, 1),
    ("relay", "m", 3, 0),
    ("take", "e", 1, 0, 1),
    ("compute", (2, 2), 1),
    ("relay", "b", 0, 0),
    ("relay", "b", 1, 0),
    ("relay", "e", 1, 1),
    ("give", (3, 3), 0),
    ("take", "e", 1, 1, 1),
    ("relay", "m", 2, 0),
    ("take", "e", 1, 0, 0),
    ("relay", "e", 2, 0),
    ("compute", (1, 0), 0),
    ("give", (2, 2), 0),
    ("relay", "e", 2, 1),
    ("give", (2, 0), 1),
    ("relay", "m", 2, 1),
    ("shared", 0),
    ("own", 0),
    ("relay", "e", 1, 0),
    ("relay", "m", 0, 0),
    ("give", (1, 2), 1),
    ("give", (1, 0), 0),
    ("finish", 0),
    ("finish", 1),
)


def fused_kernel(
    dims,
    res_hbm,
    q_hbm,
    k_hbm,
    v_hbm,
    seg_hbm,
    routes_hbm,
    rw_hbm,
    sinks_ref,
    wo_hbm,
    gain_hbm,
    eg_hbm,
    eu_hbm,
    ed_hbm,
    sg_hbm,
    su_hbm,
    sd_hbm,
    out_ref,
    q_ref,
    k_ref,
    v_ref,
    seg_ref,
    routes_ref,
    rw_ref,
    gain_ref,
    res_v,
    wo_v,
    gu_v,
    sgu_v,
    dn_v,
    sdn_v,
    kh,
    vh,
    mh,
    marks_own,
    marks_v,
    wx,
    att,
    b1s,
    b1r,
    b2s,
    b2r,
    keep,
    upd,
    norm_v,
    act,
    ret,
    rin,
    acc,
    w_sem,
    halo_s,
    halo_r,
    x_s,
    x_r,
    b_s,
    b_r,
    c_s,
    c_r,
    u_s,
    u_r,
    a_s,
    a_r,
    e_s,
    e_r,
):
    rows, cols, width, window, hidden, heads, group = dims
    bf16, f32 = jnp.bfloat16, jnp.float32
    s = lax.axis_index("sp")
    t = lax.axis_index("tp")
    core = t % 2
    chip = t // 2
    mate = t + 1 - 2 * core
    over = t + 2 - 4 * chip
    diag = 3 - t
    side = s // 2
    middle = ((s + 1) // 2) % 2
    is_mid = middle == 1
    is_end = middle == 0
    inner = s + 1 - 2 * side
    outer = (s + 3 + 2 * side) % 4

    def index_of(block):
        end, mid = block
        b = end + middle * (mid - end)
        return b + side * (3 - 2 * b)

    def remote(src, dst, send, recv, sp, tp):
        return pltpu.make_async_remote_copy(
            src_ref=src,
            dst_ref=dst,
            send_sem=send,
            recv_sem=recv,
            device_id={"sp": sp, "tp": tp},
            device_id_type=MESH,
        )

    pending = []
    conditional = []

    def go(copy, when=None):
        if when is None:
            copy.start()
            pending.append(copy)
        else:

            @pl.when(when)
            def _():
                copy.start()

            conditional.append((when, copy))

    barrier = pltpu.get_barrier_semaphore()
    for sp, tp in ((s, mate), (s, over), (inner, t)):
        pl.semaphore_signal(barrier, inc=1, device_id={"sp": sp, "tp": tp}, device_id_type=MESH)

    @pl.when(is_mid)
    def _():
        pl.semaphore_signal(barrier, inc=1, device_id={"sp": outer, "tp": t}, device_id_type=MESH)

    own_cols = pl.ds(pl.multiple_of(t * cols, cols), cols)
    first_half = pl.ds(0, hidden)
    second_half = pl.ds(hidden, hidden)
    sources = dict(
        seg=(seg_hbm, seg_ref),
        k=(k_hbm, k_ref),
        q=(q_hbm, q_ref),
        v=(v_hbm, v_ref),
        routes=(routes_hbm, routes_ref),
        rw=(rw_hbm, rw_ref),
        wo=(wo_hbm, wo_v),
        res=(res_hbm.at[:, own_cols], res_v),
        gain=(gain_hbm, gain_ref),
        eg=(eg_hbm.at[0], gu_v.at[:, first_half]),
        eu=(eu_hbm.at[0], gu_v.at[:, second_half]),
        sg=(sg_hbm, sgu_v.at[:, first_half]),
        su=(su_hbm, sgu_v.at[:, second_half]),
        ed=(ed_hbm.at[0], dn_v),
        sd=(sd_hbm, sdn_v),
    )
    loads = {
        name: pltpu.make_async_copy(src, dst, w_sem.at[i])
        for i, (name, (src, dst)) in enumerate(sources.items())
    }
    early = ("seg", "k", "q", "v", "routes", "rw", "wo", "res", "gain")
    for name in early:
        loads[name].start()

    def loaded(*names):
        for name in names:
            loads[name].wait()

    tail = pl.ds(rows - window, window)
    up_sp = (s + 1) % 4
    halos = [
        remote(k_ref.at[tail], kh, halo_s.at[0], halo_r.at[0], up_sp, t),
        remote(v_ref.at[tail], vh, halo_s.at[1], halo_r.at[1], up_sp, t),
        remote(marks_v, mh, halo_s.at[2], halo_r.at[2], up_sp, t),
    ]

    @pl.when(s == 0)
    def _():
        kh[...] = jnp.zeros_like(kh)
        vh[...] = jnp.zeros_like(vh)
        mh[...] = jnp.full(mh.shape, -1.0, f32)

    loaded("seg")
    marks_own[...] = jnp.broadcast_to(seg_ref[...].astype(f32), marks_own.shape)
    marks_v[...] = marks_own[:, tail]

    def down_rows(row):
        return jnp.transpose(jnp.broadcast_to(row, (window, window)))

    q_pos = lax.broadcasted_iota(jnp.int32, (window, window), 0)
    k_pos = lax.broadcasted_iota(jnp.int32, (window, window), 1)

    def attend(n):
        here = pl.ds(n * window, window)
        if n == 0:
            k_prev, v_prev, m_prev = kh, vh, mh[0:1, :]
            before = slice(None)
        else:
            before = pl.ds((n - 1) * window, window)
            k_prev, v_prev, m_prev = k_ref, v_ref, marks_own[0:1, before]
        m_own = marks_own[0:1, here]
        marks = down_rows(m_own)
        ok_prev = (k_pos > q_pos) & (marks == m_prev)
        ok_own = (k_pos <= q_pos) & (marks == m_own)
        contract = (((1,), (1,)), ((), ()))
        every = range(heads)
        kv = [slice((h // group) * HEAD_DIM, (h // group + 1) * HEAD_DIM) for h in every]
        scores = []
        for h in every:
            qh = q_ref[here, h * HEAD_DIM : (h + 1) * HEAD_DIM]
            pair = [
                lax.dot_general(qh, k, contract, preferred_element_type=f32) * HEAD_DIM ** (-0.5)
                for k in (k_prev[before, kv[h]], k_ref[here, kv[h]])
            ]
            scores.append((jnp.where(ok_prev, pair[0], -jnp.inf), jnp.where(ok_own, pair[1], -jnp.inf)))
        tops = [
            jnp.maximum(jnp.max(jnp.maximum(*scores[h]), axis=-1, keepdims=True), sinks_ref[h])
            for h in every
        ]
        terms = [tuple(jnp.exp(score - tops[h]) for score in scores[h]) for h in every]
        totals = [
            jnp.sum(terms[h][0] + terms[h][1], axis=-1, keepdims=True)
            + jnp.exp(sinks_ref[h] - tops[h])
            for h in every
        ]
        for h in every:
            inverse = 1.0 / totals[h]
            p_prev, p_own = ((term * inverse).astype(bf16) for term in terms[h])
            got = jnp.dot(p_prev, v_prev[before, kv[h]], preferred_element_type=f32) + jnp.dot(
                p_own, v_ref[here, kv[h]], preferred_element_type=f32
            )
            att[here, h * HEAD_DIM : (h + 1) * HEAD_DIM] = got.astype(bf16)

    def project(n, chunk):
        where = pl.ds(pl.multiple_of(chunk * cols, cols), cols)
        return jnp.dot(
            att[pl.ds(n * window, window), :], wo_v[:, where], preferred_element_type=f32
        )

    part_rows = rows // PARTS
    per_half = window // part_rows

    def parts_of(n):
        return range(n * per_half, (n + 1) * per_half)

    def part_span(p):
        return pl.ds(p * part_rows, part_rows)

    first = {}
    second = {}

    def reduce_in_chip(n):
        for far in (1, 0):
            chunk = (over if far else t) + 1 - 2 * core
            b1s[n, far] = project(n, chunk).astype(bf16)
            copy = remote(
                b1s.at[n, far], b1r.at[n, far], b_s.at[n, far], b_r.at[n, far], s, mate
            )
            go(copy)
            first[n, far] = copy

    def reduce_across(n):
        mine = project(n, over)
        first[n, 1].wait_recv()
        mine = mine + b1r[n, 1].astype(f32)
        for i, p in enumerate(parts_of(n)):
            b2s[p] = mine[i * part_rows : (i + 1) * part_rows].astype(bf16)
            copy = remote(b2s.at[p], b2r.at[p], c_s.at[p], c_r.at[p], s, over)
            go(copy)
            second[p] = copy

    def hold(n):
        here = pl.ds(n * window, window)
        mine = project(n, t) + res_v[here, :].astype(f32)
        first[n, 0].wait_recv()
        keep[here, :] = mine + b1r[n, 0].astype(f32)

    def piece(b, chunk, p):
        return upd.at[b, chunk, part_span(p)]

    def share(kind, b, chunk, p, sp, tp):
        return remote(
            piece(b, chunk, p),
            piece(b, chunk, p),
            u_s.at[kind, b, p],
            u_r.at[b, chunk, p],
            sp,
            tp,
        )

    roles = dict(e=is_end, m=is_mid, b=None)

    def send_own(role, far, p, passed):
        chunk = over if passed else t
        go(share(far + 5 * passed, s, chunk, p, outer if far else inner, t), roles[role])

    def publish(p):
        second[p].wait_recv()
        upd[s, t, part_span(p), :] = (keep[part_span(p), :] + b2r[p].astype(f32)).astype(bf16)
        go(share(3, s, t, p, s, over))
        go(share(2, s, t, p, s, mate))

    def own_over(p):
        share(4, s, over, p, s, mate).wait_recv()
        go(share(4, s, over, p, s, mate))

    def onward(block):
        return inner if block == 0 else outer

    def take(role, block, p, passed):
        b = block + side * (3 - 2 * block)
        chunk = over if passed else t
        copies = []
        if role == "m" and (p in ALONG or not passed):
            copies.append(share(5 * passed, b, chunk, p, onward(block), t))
        if not passed and p not in ALONG:
            copies.append(share(3, b, chunk, p, s, over))
        copies.append(share(2 + 2 * passed, b, chunk, p, s, mate))

        @pl.when(roles[role])
        def _():
            share(0, b, chunk, p, s, mate).wait_recv()
            for copy in copies:
                copy.start()

        conditional.extend((roles[role], copy) for copy in copies)

    def normalize(block, n):
        b = index_of(block)
        for p in parts_of(n):
            share(2, b, mate, p, s, mate).wait_recv()
            share(4, b, diag, p, s, mate).wait_recv()
        step = 32

        def body(i, carry):
            here = pl.ds(pl.multiple_of(n * window + i * step, step), step)
            squares = jnp.zeros((step, 1), f32)
            for chunk in range(4):
                part = upd[b, chunk, here, :].astype(f32)
                squares = squares + jnp.sum(part * part, axis=-1, keepdims=True)
            inv = lax.rsqrt(squares / width + epsilon)
            for chunk in range(4):
                part = upd[b, chunk, here, :].astype(f32)
                span = slice(chunk * cols, (chunk + 1) * cols)
                norm_v[here, span] = (part * inv * gain_ref[0:1, span]).astype(bf16)
            return carry

        lax.fori_loop(0, window // step, body, 0)

    def slot_of(block):
        return 4 if block is None else index_of(block)

    def pass_on(slot, kind, chunk, tp, n):
        place = act.at[slot, chunk, pl.ds(n * window, window)]
        return remote(place, place, a_s.at[kind, slot, n], a_r.at[slot, chunk, n], s, tp)

    def activate(block, n):
        slot = slot_of(block)
        here = pl.ds(n * window, window)
        weight = sgu_v if block is None else gu_v
        both = jnp.dot(norm_v[here, :], weight[...], preferred_element_type=f32)
        gate, lin = both[:, :hidden], both[:, hidden:]
        act[slot, t, here, :] = (gate / (1.0 + jnp.exp(-gate)) * lin).astype(bf16)
        go(pass_on(slot, 0, t, over, n))
        go(pass_on(slot, 1, t, mate, n))

    def relay_act(role, block, n):
        if role == "b":
            copy = pass_on(s if block == 0 else 4, 2, over, mate, n)
            copy.wait_recv()
            go(copy)
        else:
            copy = pass_on(block + side * (3 - 2 * block), 2, over, mate, n)

            @pl.when(roles[role])
            def _():
                copy.wait_recv()
                copy.start()

            conditional.append((roles[role], copy))

    def contract_act(block, n):
        slot = slot_of(block)
        weight = sdn_v if block is None else dn_v
        pass_on(slot, 1, mate, mate, n).wait_recv()
        pass_on(slot, 2, diag, mate, n).wait_recv()
        total = None
        for chunk in range(4):
            part = jnp.dot(
                act[slot, chunk, pl.ds(n * window, window), :],
                weight[chunk * hidden : (chunk + 1) * hidden, :],
                preferred_element_type=f32,
            )
            total = part if total is None else total + part
        return total

    def weighted(block, n, total, other):
        here = pl.ds(n * window, window)
        listed = wx[index_of(block), :, here]
        place = lax.broadcasted_iota(jnp.int32, listed.shape, 0)
        column = down_rows(jnp.sum(jnp.where(place == s, listed, 0.0), axis=0, keepdims=True))
        return [
            column * total[:, c : c + window] + other(slice(c, c + window)).astype(f32)
            for c in range(0, cols, window)
        ]

    def back(flow, b, n, sp):
        here = pl.ds(n * window, window)
        return remote(
            ret.at[b, here], rin.at[flow, b, here], e_s.at[b, n], e_r.at[flow, b, n], sp, t
        )

    def give(block, n):
        b = index_of(block)
        here = pl.ds(n * window, window)
        if block[1] == 0:
            flow, sp = side + middle * (1 - 2 * side), inner + middle * (outer - inner)
        else:
            flow, sp = side, inner
        copy = back(flow, b, n, sp)
        total = contract_act(block, n)

        @pl.when(is_mid)
        def _():
            copy.wait_recv()

        sums = weighted(block, n, total, lambda c: rin[flow, b, here, c])
        for i, value in enumerate(sums):
            ret[b, here, i * window : (i + 1) * window] = value.astype(bf16)
        go(copy)

    def keep_own(n):
        here = pl.ds(n * window, window)
        sums = weighted(OWN, n, contract_act(OWN, n), lambda c: upd[s, t, here, c])
        for i, value in enumerate(sums):
            span = slice(i * window, (i + 1) * window)
            acc[here, span] = acc[here, span] + value

    def keep_shared(n):
        acc[pl.ds(n * window, window), :] = contract_act(None, n)

    def gather_in(n):
        here = pl.ds(n * window, window)
        back(1 - side, s, n, inner).wait_recv()

        @pl.when(is_mid)
        def _():
            back(side, s, n, outer).wait_recv()

        out_ref[here, :] = (
            acc[here, :] + rin[0, s, here, :].astype(f32) + rin[1, s, here, :].astype(f32)
        ).astype(bf16)

    def weights_on(kind, b, sp):
        return remote(wx.at[b], wx.at[b], x_s.at[kind], x_r.at[b], sp, t)

    def take_weights(role, block):
        copy = weights_on(2 + block, block + side * (3 - 2 * block), onward(block))

        @pl.when(roles[role])
        def _():
            copy.wait_recv()
            if role == "m":
                copy.start()

        if role == "m":
            conditional.append((is_mid, copy))

    def compute(block, n):
        normalize(block, n)
        activate(block, n)

    def compute_own(n):
        compute(OWN, n)
        activate(None, n)

    def enter():
        loaded("routes", "rw")
        wx[s] = jnp.zeros(wx.shape[1:], f32)
        for e in range(4):
            weight = jnp.zeros((1, rows), f32)
            for k in range(routes_ref.shape[0]):
                named = routes_ref[k : k + 1, :] == e
                weight = weight + jnp.where(named, rw_ref[k : k + 1, :], 0.0)
            wx[s, e : e + 1, :] = weight
        pl.semaphore_wait(barrier, 3 + middle)

        @pl.when(s < 3)
        def _():
            for copy in halos:
                copy.start()

        go(weights_on(0, s, inner))
        go(weights_on(1, s, outer), is_mid)
        loaded("wo")

    def load_rest():
        for name in loads:
            if name not in early:
                loads[name].start()

        @pl.when(is_end)
        def _():
            rin[side] = jnp.zeros(rin.shape[1:], bf16)

    def halo():
        @pl.when(s > 0)
        def _():
            for copy in halos:
                copy.wait_recv()

    steps = dict(
        attend=attend,
        enter=enter,
        rest=load_rest,
        halo=halo,
        chip=reduce_in_chip,
        across=reduce_across,
        hold=hold,
        loaded=loaded,
        publish=publish,
        send=send_own,
        own_over=own_over,
        take=take,
        weights=take_weights,
        compute=compute,
        compute_own=compute_own,
        relay=relay_act,
        give=give,
        shared=keep_shared,
        own=keep_own,
        finish=gather_in,
    )
    loaded("k", "q", "v")
    for name, *given in STEPS:
        steps[name](*given)

    for copy in pending:
        copy.wait_send()
    for when, copy in conditional:

        @pl.when(when)
        def _():
            copy.wait_send()

    @pl.when(s < 3)
    def _():
        for copy in halos:
            copy.wait_send()


def layer(
    residual,
    queries,
    keys,
    values,
    segments,
    routes,
    route_weight,
    sinks,
    out_weight,
    norm_gain,
    expert_gate,
    expert_up,
    expert_down,
    shared_gate,
    shared_up,
    shared_down,
):
    arguments = (
        residual,
        queries,
        keys,
        values,
        segments,
        routes,
        route_weight,
        sinks,
        out_weight,
        norm_gain,
        expert_gate,
        expert_up,
        expert_down,
        shared_gate,
        shared_up,
        shared_down,
    )
    rows, width = residual.shape
    n_sp, n_tp = lax.axis_size("sp"), lax.axis_size("tp")
    capacity = 2 * rows * routes.shape[1] // n_sp
    hidden = expert_gate.shape[2]
    if n_sp != 4 or n_tp != 4 or capacity < rows or rows != 2 * WINDOW or shared_gate.shape[1] != hidden:
        return shards(*arguments)
    cols = width // n_tp
    heads = queries.shape[1] // HEAD_DIM
    group = queries.shape[1] // keys.shape[1]
    kv_width = keys.shape[1]
    blocks = rows // WINDOW
    bf16, f32 = jnp.bfloat16, jnp.float32
    vmem = pl.BlockSpec(memory_space=pltpu.VMEM)
    anywhere = pl.BlockSpec(memory_space=pl.ANY)
    dma = pltpu.SemaphoreType.DMA
    piece = rows // PARTS
    return pl.pallas_call(
        functools.partial(fused_kernel, (rows, cols, width, WINDOW, hidden, heads, group)),
        out_shape=jax.ShapeDtypeStruct((rows, cols), bf16),
        in_specs=[anywhere] * 7 + [pl.BlockSpec(memory_space=pltpu.SMEM)] + [anywhere] * 8,
        out_specs=vmem,
        scratch_shapes=[
            pltpu.VMEM(queries.shape, bf16),
            pltpu.VMEM(keys.shape, bf16),
            pltpu.VMEM(values.shape, bf16),
            pltpu.VMEM((1, rows), jnp.int32),
            pltpu.VMEM(routes.shape[::-1], jnp.int32),
            pltpu.VMEM(routes.shape[::-1], f32),
            pltpu.VMEM((1, width), f32),
            pltpu.VMEM((rows, cols), bf16),
            pltpu.VMEM(out_weight.shape, bf16),
            pltpu.VMEM((width, 2 * hidden), bf16),
            pltpu.VMEM((width, 2 * hidden), bf16),
            pltpu.VMEM(expert_down.shape[1:], bf16),
            pltpu.VMEM(shared_down.shape, bf16),
            pltpu.VMEM((WINDOW, kv_width), bf16),
            pltpu.VMEM((WINDOW, kv_width), bf16),
            pltpu.VMEM((8, WINDOW), f32),
            pltpu.VMEM((8, rows), f32),
            pltpu.VMEM((8, WINDOW), f32),
            pltpu.VMEM((4, 8, rows), f32),
            pltpu.VMEM((rows, heads * HEAD_DIM), bf16),
            pltpu.VMEM((blocks, 2, WINDOW, cols), bf16),
            pltpu.VMEM((blocks, 2, WINDOW, cols), bf16),
            pltpu.VMEM((PARTS, piece, cols), bf16),
            pltpu.VMEM((PARTS, piece, cols), bf16),
            pltpu.VMEM((rows, cols), f32),
            pltpu.VMEM((4, 4, rows, cols), bf16),
            pltpu.VMEM((rows, width), bf16),
            pltpu.VMEM((5, 4, rows, hidden), bf16),
            pltpu.VMEM((4, rows, cols), bf16),
            pltpu.VMEM((2, 4, rows, cols), bf16),
            pltpu.VMEM((rows, cols), f32),
            dma((16,)),
            dma((3,)),
            dma((3,)),
            dma((6,)),
            dma((4,)),
            dma((blocks, 2)),
            dma((blocks, 2)),
            dma((PARTS,)),
            dma((PARTS,)),
            dma((7, 4, PARTS)),
            dma((4, 4, PARTS)),
            dma((3, 5, blocks)),
            dma((5, 4, blocks)),
            dma((4, blocks)),
            dma((2, 4, blocks)),
        ],
        compiler_params=pltpu.CompilerParams(collective_id=0, has_side_effects=True),
    )(
        residual,
        queries,
        keys,
        values,
        segments[None, :],
        routes.T,
        route_weight.T,
        sinks,
        out_weight,
        norm_gain[None, :],
        expert_gate,
        expert_up,
        expert_down,
        shared_gate,
        shared_up,
        shared_down,
    )


def solution(mesh):
    placed = (
        P(("grp", "sp"), None),
        P(("grp", "sp"), "tp"),
        P(("grp", "sp"), "tp"),
        P(("grp", "sp"), "tp"),
        P(("grp", "sp")),
        P(("grp", "sp"), None),
        P(("grp", "sp"), None),
        P("tp"),
        P("tp", None),
        P(),
        P("sp", None, "tp"),
        P("sp", None, "tp"),
        P("sp", None, "tp"),
        P(None, "tp"),
        P(None, "tp"),
        P(None, "tp"),
    )
    return jax.shard_map(
        layer, mesh=mesh, in_specs=placed, out_specs=P(("grp", "sp"), "tp"), check_vma=False
    )
```

time: 70.1 us -> 62.7 us (0.89)
  Pallas kernels: 68.3 us -> 60.9 us
    pallas_call x1, Pallas kernels: 68.3 us -> 60.9 us  [layer(): pl.pallas_call(functools.partial(fused_kernel, (rows, cols, width, WINDOW...]
where the time goes in v1:
time: 62.7 us; the launch traced here: 62.5 us
  Pallas kernels  60.9 us (97%)
  local copies, waits for them, and re-layouts  1.67 us (3%)
    pallas_call x1, Pallas kernels, layer(): pl.pallas_call(functools.partial(fused_kernel, (rows, cols, width, WINDOW...  60.9 us
    unnamed x1, local copies, waits for them, and re-layouts  1.67 us

profile of v1, /device:TPU:0, one launch (start us, length us, event | category | flops | bytes accessed | tf_op | source)
XLA Modules:
  0.0 62.5 jit_solution(4987165144069227000)
XLA Ops:
  0.0 60.9 %shard_map.154 = bf16[256,512]{1,0:T(8,128)(2,1)} custom-call(bf16[256,2048]{1,0:T(8,128)(2,1)} %res_hbm.1, bf16[256,256]{1,0:T(8,128)(2,1)} %q_hbm.1, bf16[256,128]{1,0:T(8,128)(2,1)} %k_hbm.1, bf16[256,128]{1,0:T(8,128)(2,1)} %v_hbm.1, s32[1,256]{1,0:T(1,128)} %bitcast.7, s32[2,256]{1,0:T(2,128)} %bitcast.5, f32[2,256]{1,0:T(2,128)} %bitcast.6, ...), custom_call_target="tpu_custom_call" | custom-call | tf_op jit(solution)/shard_map/pallas_call | solution.py:874
  60.9 1.7 %copy.18 = bf16[256,512]{1,0:T(8,128)(2,1)} copy(bf16[256,512]{1,0:T(8,128)(2,1)} %shard_map.154) | data formatting | bytes 524288

commit v2 on v1

--- a/solution.py
+++ b/solution.py
@@ -1,4 +1,5 @@
 import functools
+import math
 import jax
 import jax.numpy as jnp
 from jax import lax
@@ -149,139 +150,16 @@
 
 MESH = pl.DeviceIdType.MESH
 PARTS = 4
-ALONG = (0, 2)
 OWN = (0, 1)
-STEPS = (
-    ("attend", 1),
-    ("loaded", "res"),
-    ("enter",),
-    ("chip", 1),
-    ("across", 1),
-    ("hold", 1),
-    ("halo",),
-    ("attend", 0),
-    ("publish", 2),
-    ("send", "e", 0, 2, 0),
-    ("weights", "m", 0),
-    ("send", "m", 1, 2, 0),
-    ("chip", 0),
-    ("across", 0),
-    ("rest",),
-    ("publish", 3),
-    ("weights", "m", 2),
-    ("send", "m", 1, 3, 0),
-    ("send", "m", 0, 3, 0),
-    ("take", "m", 0, 2, 0),
-    ("send", "e", 0, 3, 0),
-    ("hold", 0),
-    ("own_over", 2),
-    ("send", "e", 0, 2, 1),
-    ("send", "m", 1, 2, 1),
-    ("take", "m", 0, 3, 0),
-    ("loaded", "gain", "eg", "eu", "sg", "su", "ed", "sd"),
-    ("publish", 0),
-    ("send", "m", 0, 0, 0),
-    ("take", "m", 2, 3, 0),
-    ("send", "e", 0, 0, 0),
-    ("publish", 1),
-    ("send", "e", 0, 1, 0),
-    ("weights", "e", 3),
-    ("weights", "m", 3),
-    ("send", "m", 0, 1, 0),
-    ("take", "e", 2, 3, 0),
-    ("take", "m", 0, 2, 1),
-    ("send", "m", 1, 1, 0),
-    ("take", "m", 3, 3, 0),
-    ("take", "e", 1, 3, 0),
-    ("take", "m", 0, 1, 0),
-    ("take", "m", 0, 0, 0),
-    ("take", "m", 0, 3, 1),
-    ("own_over", 3),
-    ("take", "m", 3, 2, 0),
-    ("own_over", 0),
-    ("send", "e", 0, 0, 1),
-    ("take", "e", 3, 3, 0),
-    ("take", "m", 2, 1, 0),
-    ("take", "m", 3, 2, 1),
-    ("take", "e", 1, 2, 1),
-    ("compute_own", 1),
-    ("take", "e", 1, 3, 1),
-    ("own_over", 1),
-    ("take", "e", 3, 2, 0),
-    ("take", "e", 1, 2, 0),
-    ("take", "m", 3, 1, 0),
-    ("take", "m", 2, 0, 0),
-    ("take", "m", 0, 0, 1),
-    ("take", "m", 3, 3, 1),
-    ("take", "e", 2, 1, 0),
-    ("take", "e", 3, 1, 0),
-    ("take", "e", 3, 3, 1),
-    ("compute_own", 0),
-    ("take", "m", 2, 3, 1),
-    ("take", "e", 3, 2, 1),
-    ("weights", "e", 2),
-    ("send", "m", 0, 0, 1),
-    ("take", "m", 3, 0, 0),
-    ("send", "m", 0, 2, 0),
-    ("compute", (3, 0), 1),
-    ("take", "m", 3, 0, 1),
-    ("take", "e", 2, 3, 1),
-    ("take", "e", 3, 0, 0),
-    ("relay", "b", 0, 1),
-    ("send", "m", 0, 2, 1),
-    ("take", "m", 2, 1, 1),
-    ("take", "m", 2, 0, 1),
-    ("weights", "e", 1),
-    ("relay", "b", 1, 1),
-    ("take", "m", 2, 2, 0),
-    ("take", "m", 2, 2, 1),
-    ("take", "e", 3, 1, 1),
-    ("send", "m", 1, 0, 1),
-    ("take", "e", 3, 0, 1),
-    ("compute", (1, 3), 1),
-    ("take", "e", 2, 0, 0),
-    ("take", "e", 2, 0, 1),
-    ("send", "m", 1, 0, 0),
-    ("take", "e", 2, 1, 1),
-    ("take", "m", 3, 1, 1),
-    ("compute", (3, 3), 0),
-    ("take", "e", 1, 1, 0),
-    ("shared", 1),
-    ("relay", "m", 3, 1),
-    ("take", "m", 0, 1, 1),
-    ("relay", "e", 3, 1),
-    ("take", "e", 2, 2, 0),
-    ("compute", (2, 2), 0),
-    ("give", (3, 3), 1),
-    ("own", 1),
-    ("take", "e", 2, 2, 1),
-    ("relay", "e", 3, 0),
-    ("relay", "m", 0, 1),
-    ("relay", "m", 3, 0),
-    ("take", "e", 1, 0, 1),
-    ("compute", (2, 2), 1),
-    ("relay", "b", 0, 0),
-    ("relay", "b", 1, 0),
-    ("relay", "e", 1, 1),
-    ("give", (3, 3), 0),
-    ("take", "e", 1, 1, 1),
-    ("relay", "m", 2, 0),
-    ("take", "e", 1, 0, 0),
-    ("relay", "e", 2, 0),
-    ("compute", (1, 0), 0),
-    ("give", (2, 2), 0),
-    ("relay", "e", 2, 1),
-    ("give", (2, 0), 1),
-    ("relay", "m", 2, 1),
-    ("shared", 0),
-    ("own", 0),
-    ("relay", "e", 1, 0),
-    ("relay", "m", 0, 0),
-    ("give", (1, 2), 1),
-    ("give", (1, 0), 0),
-    ("finish", 0),
-    ("finish", 1),
-)
+E, M, B = 0, 1, 2
+ALONG = {
+    (E, 1): (0, 1),
+    (E, 2): (1,),
+    (E, 3): (2,),
+    (M, 0): (0, 1, 2, 3),
+    (M, 2): (1, 2),
+    (M, 3): (),
+}
 
 
 def fused_kernel(
@@ -302,7 +180,7 @@
     sg_hbm,
     su_hbm,
     sd_hbm,
-    out_ref,
+    out_hbm,
     q_ref,
     k_ref,
     v_ref,
@@ -330,24 +208,23 @@
     keep,
     upd,
     norm_v,
+    norm_h,
     act,
+    tot,
     ret,
     rin,
     acc,
+    result,
     w_sem,
-    halo_s,
+    sent_s,
+    out_s,
     halo_r,
-    x_s,
     x_r,
-    b_s,
     b_r,
-    c_s,
     c_r,
-    u_s,
     u_r,
-    a_s,
+    m_r,
     a_r,
-    e_s,
     e_r,
 ):
     rows, cols, width, window, hidden, heads, group = dims
@@ -371,30 +248,33 @@
         b = end + middle * (mid - end)
         return b + side * (3 - 2 * b)
 
-    def remote(src, dst, send, recv, sp, tp):
+    roles = (is_end, is_mid, None)
+    sent = [0, 0, 0]
+
+    def remote(src, dst, recv, sp, tp, role=B):
         return pltpu.make_async_remote_copy(
             src_ref=src,
             dst_ref=dst,
-            send_sem=send,
+            send_sem=sent_s.at[role],
             recv_sem=recv,
             device_id={"sp": sp, "tp": tp},
             device_id_type=MESH,
         )
 
-    pending = []
-    conditional = []
-
-    def go(copy, when=None):
-        if when is None:
+    def count(copy, role):
+        width_of = 2 if copy.src_ref.dtype == bf16 else 4
+        sent[role] += math.prod(copy.src_ref.shape) * width_of
+
+    def go(copy, role=B):
+        if role == B:
             copy.start()
-            pending.append(copy)
         else:
 
-            @pl.when(when)
+            @pl.when(roles[role])
             def _():
                 copy.start()
 
-            conditional.append((when, copy))
+        count(copy, role)
 
     barrier = pltpu.get_barrier_semaphore()
     for sp, tp in ((s, mate), (s, over), (inner, t)):
@@ -428,9 +308,8 @@
         name: pltpu.make_async_copy(src, dst, w_sem.at[i])
         for i, (name, (src, dst)) in enumerate(sources.items())
     }
-    early = ("seg", "k", "q", "v", "routes", "rw", "wo", "res", "gain")
-    for name in early:
-        loads[name].start()
+    for load in loads.values():
+        load.start()
 
     def loaded(*names):
         for name in names:
@@ -439,9 +318,9 @@
     tail = pl.ds(rows - window, window)
     up_sp = (s + 1) % 4
     halos = [
-        remote(k_ref.at[tail], kh, halo_s.at[0], halo_r.at[0], up_sp, t),
-        remote(v_ref.at[tail], vh, halo_s.at[1], halo_r.at[1], up_sp, t),
-        remote(marks_v, mh, halo_s.at[2], halo_r.at[2], up_sp, t),
+        remote(k_ref.at[tail], kh, halo_r.at[0], up_sp, t, 3),
+        remote(v_ref.at[tail], vh, halo_r.at[1], up_sp, t, 3),
+        remote(marks_v, mh, halo_r.at[2], up_sp, t, 3),
     ]
 
     @pl.when(s == 0)
@@ -524,7 +403,7 @@
             chunk = (over if far else t) + 1 - 2 * core
             b1s[n, far] = project(n, chunk).astype(bf16)
             copy = remote(
-                b1s.at[n, far], b1r.at[n, far], b_s.at[n, far], b_r.at[n, far], s, mate
+                b1s.at[n, far], b1r.at[n, far], b_r.at[n, far], s, mate
             )
             go(copy)
             first[n, far] = copy
@@ -535,7 +414,7 @@
         mine = mine + b1r[n, 1].astype(f32)
         for i, p in enumerate(parts_of(n)):
             b2s[p] = mine[i * part_rows : (i + 1) * part_rows].astype(bf16)
-            copy = remote(b2s.at[p], b2r.at[p], c_s.at[p], c_r.at[p], s, over)
+            copy = remote(b2s.at[p], b2r.at[p], c_r.at[p], s, over)
             go(copy)
             second[p] = copy
 
@@ -548,31 +427,30 @@
     def piece(b, chunk, p):
         return upd.at[b, chunk, part_span(p)]
 
-    def share(kind, b, chunk, p, sp, tp):
-        return remote(
-            piece(b, chunk, p),
-            piece(b, chunk, p),
-            u_s.at[kind, b, p],
-            u_r.at[b, chunk, p],
-            sp,
-            tp,
-        )
-
-    roles = dict(e=is_end, m=is_mid, b=None)
+    def share(passed, b, chunk, p, sp, tp, role=B):
+        place = piece(b, chunk, p)
+        return remote(place, place, u_r.at[b, passed, p], sp, tp, role)
+
+    def to_mate(b, chunk, p, role=B):
+        place = piece(b, chunk, p)
+        return remote(place, place, m_r.at[b, p // per_half], s, mate, role)
 
     def send_own(role, far, p, passed):
+        wanted = (M, 0) if role == E else (E, 1) if far else (M, 2)
+        if passed and p not in ALONG[wanted]:
+            return
         chunk = over if passed else t
-        go(share(far + 5 * passed, s, chunk, p, outer if far else inner, t), roles[role])
+        go(share(passed, s, chunk, p, outer if far else inner, t, role), role)
 
     def publish(p):
         second[p].wait_recv()
         upd[s, t, part_span(p), :] = (keep[part_span(p), :] + b2r[p].astype(f32)).astype(bf16)
-        go(share(3, s, t, p, s, over))
-        go(share(2, s, t, p, s, mate))
+        go(share(1, s, t, p, s, over))
+        go(to_mate(s, t, p))
 
     def own_over(p):
-        share(4, s, over, p, s, mate).wait_recv()
-        go(share(4, s, over, p, s, mate))
+        share(1, s, over, p, s, over).wait_recv()
+        go(to_mate(s, over, p))
 
     def onward(block):
         return inner if block == 0 else outer
@@ -581,25 +459,25 @@
         b = block + side * (3 - 2 * block)
         chunk = over if passed else t
         copies = []
-        if role == "m" and (p in ALONG or not passed):
-            copies.append(share(5 * passed, b, chunk, p, onward(block), t))
-        if not passed and p not in ALONG:
-            copies.append(share(3, b, chunk, p, s, over))
-        copies.append(share(2 + 2 * passed, b, chunk, p, s, mate))
+        if role == M and (not passed or p in ALONG[(M, 3) if block == 0 else (E, block)]):
+            copies.append(share(passed, b, chunk, p, onward(block), t, role))
+        if not passed and p not in ALONG[role, block]:
+            copies.append(share(1, b, chunk, p, s, over, role))
+        copies.append(to_mate(b, chunk, p, role))
 
         @pl.when(roles[role])
         def _():
-            share(0, b, chunk, p, s, mate).wait_recv()
+            share(passed, b, chunk, p, s, mate).wait_recv()
             for copy in copies:
                 copy.start()
 
-        conditional.extend((roles[role], copy) for copy in copies)
-
-    def normalize(block, n):
+        for copy in copies:
+            count(copy, role)
+
+    def normalize(block, n, rows_out):
         b = index_of(block)
-        for p in parts_of(n):
-            share(2, b, mate, p, s, mate).wait_recv()
-            share(4, b, diag, p, s, mate).wait_recv()
+        landed = upd.at[b, pl.ds(0, 2), pl.ds(n * window, window)]
+        remote(landed, landed, m_r.at[b, n], s, mate).wait_recv()
         step = 32
 
         def body(i, carry):
@@ -612,7 +490,7 @@
             for chunk in range(4):
                 part = upd[b, chunk, here, :].astype(f32)
                 span = slice(chunk * cols, (chunk + 1) * cols)
-                norm_v[here, span] = (part * inv * gain_ref[0:1, span]).astype(bf16)
+                rows_out[here, span] = (part * inv * gain_ref[0:1, span]).astype(bf16)
             return carry
 
         lax.fori_loop(0, window // step, body, 0)
@@ -620,40 +498,42 @@
     def slot_of(block):
         return 4 if block is None else index_of(block)
 
-    def pass_on(slot, kind, chunk, tp, n):
+    def pass_on(slot, chunk, tp, n, role=B):
         place = act.at[slot, chunk, pl.ds(n * window, window)]
-        return remote(place, place, a_s.at[kind, slot, n], a_r.at[slot, chunk, n], s, tp)
-
-    def activate(block, n):
+        flow = 0 if tp is over else 1
+        return remote(place, place, a_r.at[slot, flow, n], s, tp, role)
+
+    def activate(block, n, normed):
         slot = slot_of(block)
         here = pl.ds(n * window, window)
         weight = sgu_v if block is None else gu_v
-        both = jnp.dot(norm_v[here, :], weight[...], preferred_element_type=f32)
+        both = jnp.dot(normed[here, :], weight[...], preferred_element_type=f32)
         gate, lin = both[:, :hidden], both[:, hidden:]
         act[slot, t, here, :] = (gate / (1.0 + jnp.exp(-gate)) * lin).astype(bf16)
-        go(pass_on(slot, 0, t, over, n))
-        go(pass_on(slot, 1, t, mate, n))
+        go(pass_on(slot, t, over, n))
+        go(pass_on(slot, t, mate, n))
 
     def relay_act(role, block, n):
-        if role == "b":
-            copy = pass_on(s if block == 0 else 4, 2, over, mate, n)
-            copy.wait_recv()
-            go(copy)
+        if role == B:
+            slot = s if block == 0 else 4
+            pass_on(slot, over, over, n).wait_recv()
+            go(pass_on(slot, over, mate, n))
         else:
-            copy = pass_on(block + side * (3 - 2 * block), 2, over, mate, n)
+            slot = block + side * (3 - 2 * block)
+            copy = pass_on(slot, over, mate, n, role)
 
             @pl.when(roles[role])
             def _():
-                copy.wait_recv()
+                pass_on(slot, over, over, n).wait_recv()
                 copy.start()
 
-            conditional.append((roles[role], copy))
+            count(copy, role)
 
     def contract_act(block, n):
         slot = slot_of(block)
         weight = sdn_v if block is None else dn_v
-        pass_on(slot, 1, mate, mate, n).wait_recv()
-        pass_on(slot, 2, diag, mate, n).wait_recv()
+        landed = act.at[slot, pl.ds(0, 2), pl.ds(n * window, window)]
+        remote(landed, landed, a_r.at[slot, 1, n], s, mate).wait_recv()
         total = None
         for chunk in range(4):
             part = jnp.dot(
@@ -664,85 +544,96 @@
             total = part if total is None else total + part
         return total
 
-    def weighted(block, n, total, other):
+    def weighted(block, n, place, other):
         here = pl.ds(n * window, window)
+        total = contract_act(block, n)
         listed = wx[index_of(block), :, here]
-        place = lax.broadcasted_iota(jnp.int32, listed.shape, 0)
-        column = down_rows(jnp.sum(jnp.where(place == s, listed, 0.0), axis=0, keepdims=True))
-        return [
-            column * total[:, c : c + window] + other(slice(c, c + window)).astype(f32)
-            for c in range(0, cols, window)
-        ]
-
-    def back(flow, b, n, sp):
+        row = lax.broadcasted_iota(jnp.int32, listed.shape, 0)
+        column = down_rows(jnp.sum(jnp.where(row == s, listed, 0.0), axis=0, keepdims=True))
+        for c in range(0, cols, window):
+            value = column * total[:, c : c + window]
+            if other is not None:
+                value = value + other(slice(c, c + window))
+            place[here, c : c + window] = value
+
+    def back(place, b, p, sp, role=B):
+        here = part_span(p)
+        return remote(ret.at[b, here], rin.at[place, here], e_r.at[place, p], sp, t, role)
+
+    def give(block, n):
+        weighted(block, n, tot.at[index_of(block)], None)
+
+    def pass_back(role, block, p):
+        b = block + side * (3 - 2 * block)
+        here = part_span(p)
+        place = 4 if (role, block) == (E, 1) else b
+        copy = back(place, b, p, outer if (role, block) == (M, 0) else inner, role)
+
+        @pl.when(roles[role])
+        def _():
+            value = tot[b, here, :]
+            if role == M:
+                back(b, b, p, inner).wait_recv()
+                value = value + rin[b, here, :].astype(f32)
+            ret[b, here, :] = value.astype(bf16)
+            copy.start()
+
+        count(copy, role)
+
+    def keep_own(n):
         here = pl.ds(n * window, window)
-        return remote(
-            ret.at[b, here], rin.at[flow, b, here], e_s.at[b, n], e_r.at[flow, b, n], sp, t
-        )
-
-    def give(block, n):
-        b = index_of(block)
-        here = pl.ds(n * window, window)
-        if block[1] == 0:
-            flow, sp = side + middle * (1 - 2 * side), inner + middle * (outer - inner)
-        else:
-            flow, sp = side, inner
-        copy = back(flow, b, n, sp)
-        total = contract_act(block, n)
+        weighted(OWN, n, acc, lambda c: upd[s, t, here, c].astype(f32) + acc[here, c])
+
+    def keep_shared(n):
+        acc[pl.ds(n * window, window), :] = contract_act(None, n)
+
+    def gather_in(p):
+        here = part_span(p)
+        back(s, s, p, inner).wait_recv()
 
         @pl.when(is_mid)
         def _():
-            copy.wait_recv()
-
-        sums = weighted(block, n, total, lambda c: rin[flow, b, here, c])
-        for i, value in enumerate(sums):
-            ret[b, here, i * window : (i + 1) * window] = value.astype(bf16)
-        go(copy)
-
-    def keep_own(n):
-        here = pl.ds(n * window, window)
-        sums = weighted(OWN, n, contract_act(OWN, n), lambda c: upd[s, t, here, c])
-        for i, value in enumerate(sums):
-            span = slice(i * window, (i + 1) * window)
-            acc[here, span] = acc[here, span] + value
-
-    def keep_shared(n):
-        acc[pl.ds(n * window, window), :] = contract_act(None, n)
-
-    def gather_in(n):
-        here = pl.ds(n * window, window)
-        back(1 - side, s, n, inner).wait_recv()
-
-        @pl.when(is_mid)
-        def _():
-            back(side, s, n, outer).wait_recv()
-
-        out_ref[here, :] = (
-            acc[here, :] + rin[0, s, here, :].astype(f32) + rin[1, s, here, :].astype(f32)
+            back(4, s, p, outer).wait_recv()
+
+        result[here, :] = (
+            acc[here, :] + rin[s, here, :].astype(f32) + rin[4, here, :].astype(f32)
         ).astype(bf16)
-
-    def weights_on(kind, b, sp):
-        return remote(wx.at[b], wx.at[b], x_s.at[kind], x_r.at[b], sp, t)
+        stores[p].start()
+
+    stores = [
+        pltpu.make_async_copy(
+            result.at[part_span(p)], out_hbm.at[part_span(p)], out_s.at[p]
+        )
+        for p in range(PARTS)
+    ]
+
+    def weights_on(b, sp, role=B):
+        return remote(wx.at[b], wx.at[b], x_r.at[b], sp, t, role)
 
     def take_weights(role, block):
-        copy = weights_on(2 + block, block + side * (3 - 2 * block), onward(block))
+        copy = weights_on(block + side * (3 - 2 * block), onward(block), M)
 
         @pl.when(roles[role])
         def _():
             copy.wait_recv()
-            if role == "m":
+            if role == M:
                 copy.start()
 
-        if role == "m":
-            conditional.append((is_mid, copy))
+        if role == M:
+            count(copy, M)
 
     def compute(block, n):
-        normalize(block, n)
-        activate(block, n)
-
-    def compute_own(n):
-        compute(OWN, n)
-        activate(None, n)
+        normalize(block, n, norm_v)
+        activate(block, n, norm_v)
+
+    def norm_own(n):
+        normalize(OWN, n, norm_h)
+
+    def act_own(n):
+        activate(OWN, n, norm_h)
+
+    def act_shared(n):
+        activate(None, n, norm_h)
 
     def enter():
         loaded("routes", "rw")
@@ -760,18 +651,14 @@
             for copy in halos:
                 copy.start()
 
-        go(weights_on(0, s, inner))
-        go(weights_on(1, s, outer), is_mid)
+        go(weights_on(s, inner))
+        go(weights_on(s, outer, M), M)
         loaded("wo")
 
-    def load_rest():
-        for name in loads:
-            if name not in early:
-                loads[name].start()
-
+    def clear():
         @pl.when(is_end)
         def _():
-            rin[side] = jnp.zeros(rin.shape[1:], bf16)
+            rin[4] = jnp.zeros(rin.shape[1:], bf16)
 
     def halo():
         @pl.when(s > 0)
@@ -779,44 +666,193 @@
             for copy in halos:
                 copy.wait_recv()
 
-    steps = dict(
-        attend=attend,
-        enter=enter,
-        rest=load_rest,
-        halo=halo,
-        chip=reduce_in_chip,
-        across=reduce_across,
-        hold=hold,
-        loaded=loaded,
-        publish=publish,
-        send=send_own,
-        own_over=own_over,
-        take=take,
-        weights=take_weights,
-        compute=compute,
-        compute_own=compute_own,
-        relay=relay_act,
-        give=give,
-        shared=keep_shared,
-        own=keep_own,
-        finish=gather_in,
-    )
     loaded("k", "q", "v")
-    for name, *given in STEPS:
-        steps[name](*given)
-
-    for copy in pending:
-        copy.wait_send()
-    for when, copy in conditional:
-
-        @pl.when(when)
-        def _():
-            copy.wait_send()
+    attend(1)
+    enter()
+    reduce_in_chip(1)
+    loaded("res")
+    reduce_across(1)
+    hold(1)
+    take_weights(M, 2)
+    halo()
+    attend(0)
+    reduce_in_chip(0)
+    take_weights(M, 0)
+    reduce_across(0)
+    publish(2)
+    clear()
+    send_own(E, 0, 2, 0)
+    send_own(M, 0, 2, 0)
+    loaded("gain", "eg", "eu", "sg", "su", "ed", "sd")
+    send_own(M, 1, 2, 0)
+    hold(0)
+    publish(3)
+    send_own(E, 0, 3, 0)
+    send_own(M, 0, 3, 0)
+    send_own(M, 1, 3, 0)
+    take(M, 0, 2, 0)
+    take_weights(M, 3)
+    publish(0)
+    take(M, 2, 2, 0)
+    take(M, 0, 3, 0)
+    take(M, 2, 3, 0)
+    take(M, 0, 0, 0)
+    take(M, 3, 2, 0)
+    send_own(E, 0, 0, 0)
+    publish(1)
+    take(M, 0, 1, 0)
+    send_own(E, 0, 1, 0)
+    take(E, 1, 2, 0)
+    own_over(2)
+    take(M, 3, 3, 0)
+    send_own(M, 0, 0, 0)
+    send_own(E, 0, 2, 1)
+    own_over(3)
+    own_over(0)
+    send_own(E, 0, 0, 1)
+    take(E, 2, 2, 0)
+    take(M, 3, 0, 0)
+    take(E, 2, 3, 0)
+    take(M, 3, 1, 0)
+    take(M, 0, 2, 1)
+    take_weights(E, 1)
+    take_weights(E, 3)
+    take(M, 2, 3, 1)
+    send_own(M, 0, 1, 0)
+    take(M, 3, 2, 1)
+    send_own(M, 0, 2, 1)
+    take(E, 1, 3, 0)
+    take(M, 2, 0, 0)
+    own_over(1)
+    send_own(M, 0, 1, 1)
+    norm_own(1)
+    take(E, 2, 2, 1)
+    send_own(E, 0, 3, 1)
+    take_weights(E, 2)
+    take(E, 1, 2, 1)
+    send_own(M, 1, 1, 1)
+    take(E, 3, 3, 0)
+    take(E, 2, 3, 1)
+    take(M, 3, 3, 1)
+    take(E, 3, 0, 0)
+    send_own(M, 1, 0, 1)
+    take(M, 0, 0, 1)
+    take(E, 3, 1, 0)
+    take(M, 0, 3, 1)
+    compute((2, 3), 1)
+    take(E, 3, 2, 0)
+    norm_own(0)
+    take(E, 3, 2, 1)
+    take(M, 2, 2, 1)
+    take(E, 3, 3, 1)
+    take(E, 3, 0, 1)
+    take(M, 2, 1, 0)
+    take(M, 2, 1, 1)
+    take(E, 1, 3, 1)
+    take(E, 2, 0, 0)
+    send_own(M, 1, 1, 0)
+    take(M, 3, 1, 1)
+    compute((3, 0), 1)
+    take(E, 3, 1, 1)
+    send_own(M, 1, 0, 0)
+    compute((1, 2), 1)
+    relay_act(E, 2, 1)
+    take(M, 3, 0, 1)
+    send_own(E, 0, 1, 1)
+    compute((3, 3), 0)
+    relay_act(M, 3, 1)
+    give((2, 3), 1)
+    pass_back(E, 2, 3)
+    pass_back(E, 2, 2)
+    take(E, 2, 0, 1)
+    act_shared(0)
+    relay_act(M, 2, 1)
+    relay_act(E, 3, 1)
+    take(M, 2, 0, 1)
+    take(E, 2, 1, 0)
+    take(E, 2, 1, 1)
+    take(E, 1, 1, 1)
+    act_own(1)
+    take(M, 0, 1, 1)
+    give((3, 2), 1)
+    pass_back(E, 3, 3)
+    relay_act(M, 3, 0)
+    compute((2, 0), 0)
+    relay_act(E, 3, 0)
+    pass_back(E, 3, 2)
+    pass_back(M, 2, 2)
+    take(E, 1, 0, 0)
+    relay_act(M, 0, 1)
+    take(E, 1, 0, 1)
+    take(E, 1, 1, 0)
+    give((3, 3), 0)
+    pass_back(E, 3, 1)
+    relay_act(E, 1, 1)
+    pass_back(M, 3, 3)
+    pass_back(E, 3, 0)
+    compute((1, 2), 0)
+    pass_back(M, 3, 2)
+    give((1, 0), 1)
+    pass_back(E, 1, 2)
+    relay_act(E, 2, 0)
+    relay_act(M, 0, 0)
+    relay_act(B, 1, 0)
+    pass_back(M, 3, 1)
+    act_own(0)
+    give((2, 0), 0)
+    pass_back(E, 2, 1)
+    pass_back(M, 0, 3)
+    relay_act(E, 1, 0)
+    pass_back(M, 3, 0)
+    pass_back(E, 2, 0)
+    act_shared(1)
+    relay_act(M, 2, 0)
+    pass_back(M, 0, 2)
+    pass_back(M, 2, 3)
+    give((1, 2), 0)
+    pass_back(E, 1, 3)
+    pass_back(M, 0, 1)
+    pass_back(M, 2, 1)
+    pass_back(E, 1, 1)
+    keep_shared(0)
+    relay_act(B, 0, 0)
+    pass_back(M, 0, 0)
+    pass_back(M, 2, 0)
+    relay_act(B, 1, 1)
+    pass_back(E, 1, 0)
+    relay_act(B, 0, 1)
+    keep_shared(1)
+    keep_own(0)
+    keep_own(1)
+    gather_in(3)
+    gather_in(1)
+    gather_in(2)
+    gather_in(0)
+
+    def settle(size, sem):
+        for unit in (upd.at[0], upd.at[0, 0], piece(0, 0, 0), wx.at[0]):
+            of_one = math.prod(unit.shape) * (4 if unit.dtype == f32 else 2)
+            for _ in range(size // of_one):
+                pltpu.make_async_copy(unit, unit, sem).wait()
+            size = size % of_one
+
+    settle(sent[B], sent_s.at[B])
+
+    @pl.when(is_end)
+    def _():
+        settle(sent[E], sent_s.at[E])
+
+    @pl.when(is_mid)
+    def _():
+        settle(sent[M], sent_s.at[M])
 
     @pl.when(s < 3)
     def _():
         for copy in halos:
             copy.wait_send()
+
+    for store in stores:
+        store.wait()
 
 
 def layer(
@@ -875,7 +911,7 @@
         functools.partial(fused_kernel, (rows, cols, width, WINDOW, hidden, heads, group)),
         out_shape=jax.ShapeDtypeStruct((rows, cols), bf16),
         in_specs=[anywhere] * 7 + [pl.BlockSpec(memory_space=pltpu.SMEM)] + [anywhere] * 8,
-        out_specs=vmem,
+        out_specs=anywhere,
         scratch_shapes=[
             pltpu.VMEM(queries.shape, bf16),
             pltpu.VMEM(keys.shape, bf16),
@@ -904,25 +940,24 @@
             pltpu.VMEM((rows, cols), f32),
             pltpu.VMEM((4, 4, rows, cols), bf16),
             pltpu.VMEM((rows, width), bf16),
+            pltpu.VMEM((rows, width), bf16),
             pltpu.VMEM((5, 4, rows, hidden), bf16),
+            pltpu.VMEM((4, rows, cols), f32),
             pltpu.VMEM((4, rows, cols), bf16),
-            pltpu.VMEM((2, 4, rows, cols), bf16),
+            pltpu.VMEM((5, rows, cols), bf16),
             pltpu.VMEM((rows, cols), f32),
-            dma((16,)),
+            pltpu.VMEM((rows, cols), bf16),
+            dma((len(arguments) - 1,)),
+            dma((4,)),
+            dma((PARTS,)),
             dma((3,)),
-            dma((3,)),
-            dma((6,)),
             dma((4,)),
             dma((blocks, 2)),
-            dma((blocks, 2)),
             dma((PARTS,)),
-            dma((PARTS,)),
-            dma((7, 4, PARTS)),
-            dma((4, 4, PARTS)),
-            dma((3, 5, blocks)),
-            dma((5, 4, blocks)),
+            dma((4, 2, PARTS)),
             dma((4, blocks)),
-            dma((2, 4, blocks)),
+            dma((5, 2, blocks)),
+            dma((5, PARTS)),
         ],
         compiler_params=pltpu.CompilerParams(collective_id=0, has_side_effects=True),
     )(

time: 62.7 us -> 55.7 us (0.89)
  Pallas kernels: 60.9 us -> 53.8 us
    pallas_call x1, Pallas kernels: 60.9 us -> 53.8 us  [layer(): pl.pallas_call(functools.partial(fused_kernel, (rows, cols, width, WINDOW...]
where the time goes in v2:
time: 55.7 us; the launch traced here: 55.5 us
  Pallas kernels  53.8 us (97%)
  local copies, waits for them, and re-layouts  1.67 us (3%)
    pallas_call x1, Pallas kernels, layer(): pl.pallas_call(functools.partial(fused_kernel, (rows, cols, width, WINDOW...  53.8 us
    unnamed x1, local copies, waits for them, and re-layouts  1.67 us

profile of v2, /device:TPU:0, one launch (start us, length us, event | category | flops | bytes accessed | tf_op | source)
XLA Modules:
  0.0 55.5 jit_solution(4378333189798157838)
XLA Ops:
  0.0 53.8 %shard_map.154 = bf16[256,512]{1,0:T(8,128)(2,1)} custom-call(bf16[256,2048]{1,0:T(8,128)(2,1)} %res_hbm.1, bf16[256,256]{1,0:T(8,128)(2,1)} %q_hbm.1, bf16[256,128]{1,0:T(8,128)(2,1)} %k_hbm.1, bf16[256,128]{1,0:T(8,128)(2,1)} %v_hbm.1, s32[1,256]{1,0:T(1,128)} %bitcast.7, s32[2,256]{1,0:T(2,128)} %bitcast.5, f32[2,256]{1,0:T(2,128)} %bitcast.6, ...), custom_call_target="tpu_custom_call" | custom-call | tf_op jit(solution)/shard_map/pallas_call | solution.py:910
  53.8 1.7 %copy.18 = bf16[256,512]{1,0:T(8,128)(2,1)} copy(bf16[256,512]{1,0:T(8,128)(2,1)} %shard_map.154) | data formatting | bytes 524288

commit v3 on v2

--- a/solution.py
+++ b/solution.py
@@ -180,7 +180,7 @@
     sg_hbm,
     su_hbm,
     sd_hbm,
-    out_hbm,
+    result,
     q_ref,
     k_ref,
     v_ref,
@@ -214,10 +214,8 @@
     ret,
     rin,
     acc,
-    result,
     w_sem,
     sent_s,
-    out_s,
     halo_r,
     x_r,
     b_r,
@@ -598,14 +596,6 @@
         result[here, :] = (
             acc[here, :] + rin[s, here, :].astype(f32) + rin[4, here, :].astype(f32)
         ).astype(bf16)
-        stores[p].start()
-
-    stores = [
-        pltpu.make_async_copy(
-            result.at[part_span(p)], out_hbm.at[part_span(p)], out_s.at[p]
-        )
-        for p in range(PARTS)
-    ]
 
     def weights_on(b, sp, role=B):
         return remote(wx.at[b], wx.at[b], x_r.at[b], sp, t, role)
@@ -851,9 +841,6 @@
         for copy in halos:
             copy.wait_send()
 
-    for store in stores:
-        store.wait()
-
 
 def layer(
     residual,
@@ -909,9 +896,9 @@
     piece = rows // PARTS
     return pl.pallas_call(
         functools.partial(fused_kernel, (rows, cols, width, WINDOW, hidden, heads, group)),
-        out_shape=jax.ShapeDtypeStruct((rows, cols), bf16),
+        out_shape=pltpu.VMEM((rows, cols), bf16),
         in_specs=[anywhere] * 7 + [pl.BlockSpec(memory_space=pltpu.SMEM)] + [anywhere] * 8,
-        out_specs=anywhere,
+        out_specs=vmem,
         scratch_shapes=[
             pltpu.VMEM(queries.shape, bf16),
             pltpu.VMEM(keys.shape, bf16),
@@ -946,10 +933,8 @@
             pltpu.VMEM((4, rows, cols), bf16),
             pltpu.VMEM((5, rows, cols), bf16),
             pltpu.VMEM((rows, cols), f32),
-            pltpu.VMEM((rows, cols), bf16),
             dma((len(arguments) - 1,)),
             dma((4,)),
-            dma((PARTS,)),
             dma((3,)),
             dma((4,)),
             dma((blocks, 2)),

time: 55.7 us -> 54.1 us (0.971)
  local copies, waits for them, and re-layouts: 1.67 us -> 0.71 us
  Pallas kernels: 53.8 us -> 53.2 us
    unnamed x1, local copies, waits for them, and re-layouts: 1.67 us -> 0.71 us
    pallas_call x1, Pallas kernels: 53.8 us -> 53.2 us  [layer(): pl.pallas_call(functools.partial(fused_kernel, (rows, cols, width, WINDOW...]
where the time goes in v3:
time: 54.1 us; the launch traced here: 53.9 us
  Pallas kernels  53.2 us (98%)
  local copies, waits for them, and re-layouts  0.71 us (1%)
    pallas_call x1, Pallas kernels, layer(): pl.pallas_call(functools.partial(fused_kernel, (rows, cols, width, WINDOW...  53.2 us

profile of v3, /device:TPU:0, one launch (start us, length us, event | category | flops | bytes accessed | tf_op | source)
XLA Modules:
  0.0 53.9 jit_solution(3742734068166802679)
XLA Ops:
  0.0 53.2 %shard_map.154 = bf16[256,512]{1,0:T(8,128)(2,1)S(1)} custom-call(bf16[256,2048]{1,0:T(8,128)(2,1)} %res_hbm.1, bf16[256,256]{1,0:T(8,128)(2,1)} %q_hbm.1, bf16[256,128]{1,0:T(8,128)(2,1)} %k_hbm.1, bf16[256,128]{1,0:T(8,128)(2,1)} %v_hbm.1, s32[1,256]{1,0:T(1,128)} %bitcast.7, s32[2,256]{1,0:T(2,128)} %bitcast.5, f32[2,256]{1,0:T(2,128)} %bitcast.6, ...), custom_call_target="tpu_custom_call" | custom-call | tf_op jit(solution)/shard_map/pallas_call | solution.py:897
  53.2 0.7 %copy.18 = bf16[256,512]{1,0:T(8,128)(2,1)} copy(bf16[256,512]{1,0:T(8,128)(2,1)S(1)} %shard_map.154) | data formatting | bytes 524288

commit v4 on v3

--- a/solution.py
+++ b/solution.py
@@ -153,12 +153,12 @@
 OWN = (0, 1)
 E, M, B = 0, 1, 2
 ALONG = {
-    (E, 1): (0, 1),
-    (E, 2): (1,),
-    (E, 3): (2,),
+    (E, 1): (0, 1, 3),
+    (E, 2): (0,),
+    (E, 3): (1,),
     (M, 0): (0, 1, 2, 3),
-    (M, 2): (1, 2),
-    (M, 3): (),
+    (M, 2): (0, 3),
+    (M, 3): (2, 3),
 }
 
 
@@ -660,164 +660,165 @@
     attend(1)
     enter()
     reduce_in_chip(1)
-    loaded("res")
     reduce_across(1)
-    hold(1)
-    take_weights(M, 2)
+    clear()
     halo()
     attend(0)
+    loaded("res")
+    take_weights(M, 0)
     reduce_in_chip(0)
-    take_weights(M, 0)
+    hold(1)
     reduce_across(0)
     publish(2)
-    clear()
+    send_own(M, 0, 2, 0)
+    take_weights(M, 2)
     send_own(E, 0, 2, 0)
-    send_own(M, 0, 2, 0)
-    loaded("gain", "eg", "eu", "sg", "su", "ed", "sd")
     send_own(M, 1, 2, 0)
     hold(0)
     publish(3)
+    loaded("gain", "eg", "eu", "sg", "su", "ed", "sd")
+    send_own(M, 0, 3, 0)
     send_own(E, 0, 3, 0)
-    send_own(M, 0, 3, 0)
     send_own(M, 1, 3, 0)
     take(M, 0, 2, 0)
     take_weights(M, 3)
+    take(M, 2, 2, 0)
     publish(0)
-    take(M, 2, 2, 0)
+    send_own(E, 0, 0, 0)
     take(M, 0, 3, 0)
     take(M, 2, 3, 0)
     take(M, 0, 0, 0)
+    publish(1)
     take(M, 3, 2, 0)
-    send_own(E, 0, 0, 0)
-    publish(1)
     take(M, 0, 1, 0)
+    send_own(M, 0, 1, 0)
     send_own(E, 0, 1, 0)
+    send_own(M, 0, 0, 0)
+    own_over(3)
+    send_own(E, 0, 3, 1)
+    take(M, 3, 3, 0)
     take(E, 1, 2, 0)
+    take(M, 2, 2, 1)
+    take_weights(E, 3)
+    take(M, 3, 0, 0)
+    own_over(0)
     own_over(2)
-    take(M, 3, 3, 0)
-    send_own(M, 0, 0, 0)
+    send_own(M, 0, 3, 1)
+    take(E, 2, 2, 0)
     send_own(E, 0, 2, 1)
-    own_over(3)
-    own_over(0)
-    send_own(E, 0, 0, 1)
-    take(E, 2, 2, 0)
-    take(M, 3, 0, 0)
+    take(M, 0, 3, 1)
     take(E, 2, 3, 0)
+    send_own(M, 0, 0, 1)
     take(M, 3, 1, 0)
     take(M, 0, 2, 1)
-    take_weights(E, 1)
-    take_weights(E, 3)
-    take(M, 2, 3, 1)
-    send_own(M, 0, 1, 0)
-    take(M, 3, 2, 1)
-    send_own(M, 0, 2, 1)
+    take(E, 3, 2, 0)
     take(E, 1, 3, 0)
-    take(M, 2, 0, 0)
-    own_over(1)
-    send_own(M, 0, 1, 1)
-    norm_own(1)
     take(E, 2, 2, 1)
-    send_own(E, 0, 3, 1)
-    take_weights(E, 2)
-    take(E, 1, 2, 1)
-    send_own(M, 1, 1, 1)
+    take(M, 2, 1, 0)
+    send_own(M, 1, 3, 1)
+    send_own(E, 0, 0, 1)
     take(E, 3, 3, 0)
     take(E, 2, 3, 1)
+    own_over(1)
+    take(E, 3, 0, 0)
+    send_own(E, 0, 1, 1)
+    compute((2, 0), 1)
+    take(E, 3, 2, 1)
+    norm_own(1)
+    take(E, 1, 2, 1)
+    norm_own(0)
+    take(E, 3, 3, 1)
+    take(M, 3, 1, 1)
+    take(M, 2, 0, 0)
+    take(E, 2, 1, 0)
+    take(M, 2, 3, 1)
+    compute((3, 2), 1)
+    take(M, 0, 1, 1)
+    take(M, 2, 1, 1)
+    relay_act(M, 0, 1)
+    take(M, 3, 0, 1)
+    take_weights(E, 2)
+    take(M, 2, 0, 1)
+    take(E, 3, 1, 0)
+    act_shared(0)
+    take(M, 0, 0, 1)
     take(M, 3, 3, 1)
-    take(E, 3, 0, 0)
-    send_own(M, 1, 0, 1)
-    take(M, 0, 0, 1)
-    take(E, 3, 1, 0)
-    take(M, 0, 3, 1)
-    compute((2, 3), 1)
-    take(E, 3, 2, 0)
-    norm_own(0)
-    take(E, 3, 2, 1)
-    take(M, 2, 2, 1)
-    take(E, 3, 3, 1)
+    take(E, 1, 3, 1)
     take(E, 3, 0, 1)
-    take(M, 2, 1, 0)
-    take(M, 2, 1, 1)
-    take(E, 1, 3, 1)
-    take(E, 2, 0, 0)
-    send_own(M, 1, 1, 0)
-    take(M, 3, 1, 1)
-    compute((3, 0), 1)
+    relay_act(E, 2, 1)
+    send_own(M, 1, 1, 1)
     take(E, 3, 1, 1)
     send_own(M, 1, 0, 0)
-    compute((1, 2), 1)
-    relay_act(E, 2, 1)
-    take(M, 3, 0, 1)
-    send_own(E, 0, 1, 1)
+    send_own(M, 1, 1, 0)
+    give((2, 0), 1)
+    pass_back(E, 2, 3)
+    take_weights(E, 1)
     compute((3, 3), 0)
-    relay_act(M, 3, 1)
-    give((2, 3), 1)
-    pass_back(E, 2, 3)
+    take(M, 3, 2, 1)
     pass_back(E, 2, 2)
+    take(E, 2, 0, 0)
+    take(E, 2, 1, 1)
     take(E, 2, 0, 1)
-    act_shared(0)
+    send_own(M, 1, 0, 1)
+    relay_act(E, 3, 1)
     relay_act(M, 2, 1)
-    relay_act(E, 3, 1)
-    take(M, 2, 0, 1)
-    take(E, 2, 1, 0)
-    take(E, 2, 1, 1)
-    take(E, 1, 1, 1)
-    act_own(1)
-    take(M, 0, 1, 1)
+    compute((1, 3), 1)
     give((3, 2), 1)
     pass_back(E, 3, 3)
+    pass_back(E, 3, 2)
+    compute((2, 0), 0)
+    take(E, 1, 0, 0)
+    relay_act(E, 3, 0)
+    pass_back(M, 2, 3)
+    act_shared(1)
     relay_act(M, 3, 0)
-    compute((2, 0), 0)
-    relay_act(E, 3, 0)
-    pass_back(E, 3, 2)
+    relay_act(B, 1, 0)
+    give((3, 3), 0)
+    pass_back(E, 3, 0)
+    pass_back(E, 3, 1)
+    relay_act(M, 3, 1)
+    take(E, 1, 1, 1)
+    take(E, 1, 1, 0)
+    relay_act(E, 1, 1)
+    take(E, 1, 0, 1)
+    give((1, 3), 1)
+    relay_act(M, 0, 0)
+    relay_act(E, 2, 0)
+    pass_back(E, 1, 3)
+    pass_back(M, 3, 3)
+    compute((1, 2), 0)
+    keep_shared(0)
+    pass_back(M, 3, 2)
+    relay_act(B, 1, 1)
+    pass_back(M, 3, 0)
+    give((2, 0), 0)
+    pass_back(E, 2, 0)
+    pass_back(E, 2, 1)
+    pass_back(E, 1, 2)
+    pass_back(M, 0, 3)
+    pass_back(M, 3, 1)
+    act_own(1)
+    relay_act(M, 2, 0)
+    relay_act(E, 1, 0)
+    pass_back(M, 0, 2)
     pass_back(M, 2, 2)
-    take(E, 1, 0, 0)
-    relay_act(M, 0, 1)
-    take(E, 1, 0, 1)
-    take(E, 1, 1, 0)
-    give((3, 3), 0)
-    pass_back(E, 3, 1)
-    relay_act(E, 1, 1)
-    pass_back(M, 3, 3)
-    pass_back(E, 3, 0)
-    compute((1, 2), 0)
-    pass_back(M, 3, 2)
-    give((1, 0), 1)
-    pass_back(E, 1, 2)
-    relay_act(E, 2, 0)
-    relay_act(M, 0, 0)
-    relay_act(B, 1, 0)
-    pass_back(M, 3, 1)
     act_own(0)
-    give((2, 0), 0)
-    pass_back(E, 2, 1)
-    pass_back(M, 0, 3)
-    relay_act(E, 1, 0)
-    pass_back(M, 3, 0)
-    pass_back(E, 2, 0)
-    act_shared(1)
-    relay_act(M, 2, 0)
-    pass_back(M, 0, 2)
-    pass_back(M, 2, 3)
     give((1, 2), 0)
-    pass_back(E, 1, 3)
+    pass_back(M, 0, 0)
+    pass_back(E, 1, 0)
+    pass_back(M, 2, 0)
     pass_back(M, 0, 1)
+    relay_act(B, 0, 1)
+    pass_back(E, 1, 1)
     pass_back(M, 2, 1)
-    pass_back(E, 1, 1)
-    keep_shared(0)
+    keep_shared(1)
     relay_act(B, 0, 0)
-    pass_back(M, 0, 0)
-    pass_back(M, 2, 0)
-    relay_act(B, 1, 1)
-    pass_back(E, 1, 0)
-    relay_act(B, 0, 1)
-    keep_shared(1)
+    keep_own(1)
     keep_own(0)
-    keep_own(1)
+    gather_in(2)
+    gather_in(0)
     gather_in(3)
     gather_in(1)
-    gather_in(2)
-    gather_in(0)
 
     def settle(size, sem):
         for unit in (upd.at[0], upd.at[0, 0], piece(0, 0, 0), wx.at[0]):

time: 54.1 us -> 52.9 us (0.978)
  Pallas kernels: 53.2 us -> 52 us
    pallas_call x1, Pallas kernels: 53.2 us -> 52 us  [layer(): pl.pallas_call(functools.partial(fused_kernel, (rows, cols, width, WINDOW...]
where the time goes in v4:
time: 52.9 us; the launch traced here: 52.7 us
  Pallas kernels  52 us (98%)
  local copies, waits for them, and re-layouts  0.71 us (1%)
    pallas_call x1, Pallas kernels, layer(): pl.pallas_call(functools.partial(fused_kernel, (rows, cols, width, WINDOW...  52 us

profile of v4, /device:TPU:0, one launch (start us, length us, event | category | flops | bytes accessed | tf_op | source)
XLA Modules:
  0.0 52.7 jit_solution(10641722136779133094)
XLA Ops:
  0.0 52.0 %shard_map.154 = bf16[256,512]{1,0:T(8,128)(2,1)S(1)} custom-call(bf16[256,2048]{1,0:T(8,128)(2,1)} %res_hbm.1, bf16[256,256]{1,0:T(8,128)(2,1)} %q_hbm.1, bf16[256,128]{1,0:T(8,128)(2,1)} %k_hbm.1, bf16[256,128]{1,0:T(8,128)(2,1)} %v_hbm.1, s32[1,256]{1,0:T(1,128)} %bitcast.7, s32[2,256]{1,0:T(2,128)} %bitcast.5, f32[2,256]{1,0:T(2,128)} %bitcast.6, ...), custom_call_target="tpu_custom_call" | custom-call | tf_op jit(solution)/shard_map/pallas_call | solution.py:898
  52.0 0.7 %copy.18 = bf16[256,512]{1,0:T(8,128)(2,1)} copy(bf16[256,512]{1,0:T(8,128)(2,1)S(1)} %shard_map.154) | data formatting | bytes 524288

commit v5 on v4

--- a/solution.py
+++ b/solution.py
@@ -171,7 +171,7 @@
     seg_hbm,
     routes_hbm,
     rw_hbm,
-    sinks_ref,
+    sinks_hbm,
     wo_hbm,
     gain_hbm,
     eg_hbm,
@@ -187,6 +187,7 @@
     seg_ref,
     routes_ref,
     rw_ref,
+    sinks_ref,
     gain_ref,
     res_v,
     wo_v,
@@ -285,33 +286,28 @@
     own_cols = pl.ds(pl.multiple_of(t * cols, cols), cols)
     first_half = pl.ds(0, hidden)
     second_half = pl.ds(hidden, hidden)
-    sources = dict(
-        seg=(seg_hbm, seg_ref),
-        k=(k_hbm, k_ref),
-        q=(q_hbm, q_ref),
-        v=(v_hbm, v_ref),
-        routes=(routes_hbm, routes_ref),
-        rw=(rw_hbm, rw_ref),
-        wo=(wo_hbm, wo_v),
-        res=(res_hbm.at[:, own_cols], res_v),
-        gain=(gain_hbm, gain_ref),
-        eg=(eg_hbm.at[0], gu_v.at[:, first_half]),
-        eu=(eu_hbm.at[0], gu_v.at[:, second_half]),
-        sg=(sg_hbm, sgu_v.at[:, first_half]),
-        su=(su_hbm, sgu_v.at[:, second_half]),
-        ed=(ed_hbm.at[0], dn_v),
-        sd=(sd_hbm, sdn_v),
-    )
-    loads = {
-        name: pltpu.make_async_copy(src, dst, w_sem.at[i])
-        for i, (name, (src, dst)) in enumerate(sources.items())
-    }
-    for load in loads.values():
-        load.start()
-
-    def loaded(*names):
-        for name in names:
-            loads[name].wait()
+    sources = (
+        ((seg_hbm, seg_ref),),
+        ((k_hbm, k_ref), (q_hbm, q_ref), (v_hbm, v_ref)),
+        ((sinks_hbm, sinks_ref),),
+        ((routes_hbm, routes_ref),),
+        ((rw_hbm, rw_ref),),
+        ((wo_hbm, wo_v),),
+        ((res_hbm.at[:, own_cols], res_v),),
+        ((gain_hbm, gain_ref),),
+        ((eg_hbm.at[0], gu_v.at[:, first_half]), (eu_hbm.at[0], gu_v.at[:, second_half])),
+        ((sg_hbm, sgu_v.at[:, first_half]), (su_hbm, sgu_v.at[:, second_half])),
+        ((ed_hbm.at[0], dn_v), (sd_hbm, sdn_v)),
+    )
+    for i, group_of in enumerate(sources):
+        for src, dst in group_of:
+            pltpu.make_async_copy(src, dst, w_sem.at[i]).start()
+    as_large = {1: upd.at[0, 0], 8: gu_v, 9: sgu_v, 10: gu_v}
+
+    def loaded(*which):
+        for i in which:
+            whole = as_large[i] if i in as_large else sources[i][0][1]
+            pltpu.make_async_copy(whole, whole, w_sem.at[i]).wait()
 
     tail = pl.ds(rows - window, window)
     up_sp = (s + 1) % 4
@@ -327,7 +323,7 @@
         vh[...] = jnp.zeros_like(vh)
         mh[...] = jnp.full(mh.shape, -1.0, f32)
 
-    loaded("seg")
+    loaded(0)
     marks_own[...] = jnp.broadcast_to(seg_ref[...].astype(f32), marks_own.shape)
     marks_v[...] = marks_own[:, tail]
 
@@ -626,7 +622,7 @@
         activate(None, n, norm_h)
 
     def enter():
-        loaded("routes", "rw")
+        loaded(3, 4)
         wx[s] = jnp.zeros(wx.shape[1:], f32)
         for e in range(4):
             weight = jnp.zeros((1, rows), f32)
@@ -643,7 +639,7 @@
 
         go(weights_on(s, inner))
         go(weights_on(s, outer, M), M)
-        loaded("wo")
+        loaded(5)
 
     def clear():
         @pl.when(is_end)
@@ -656,7 +652,7 @@
             for copy in halos:
                 copy.wait_recv()
 
-    loaded("k", "q", "v")
+    loaded(1, 2)
     attend(1)
     enter()
     reduce_in_chip(1)
@@ -664,7 +660,7 @@
     clear()
     halo()
     attend(0)
-    loaded("res")
+    loaded(6)
     take_weights(M, 0)
     reduce_in_chip(0)
     hold(1)
@@ -676,7 +672,7 @@
     send_own(M, 1, 2, 0)
     hold(0)
     publish(3)
-    loaded("gain", "eg", "eu", "sg", "su", "ed", "sd")
+    loaded(7, 8, 9, 10)
     send_own(M, 0, 3, 0)
     send_own(E, 0, 3, 0)
     send_own(M, 1, 3, 0)
@@ -898,7 +894,7 @@
     return pl.pallas_call(
         functools.partial(fused_kernel, (rows, cols, width, WINDOW, hidden, heads, group)),
         out_shape=pltpu.VMEM((rows, cols), bf16),
-        in_specs=[anywhere] * 7 + [pl.BlockSpec(memory_space=pltpu.SMEM)] + [anywhere] * 8,
+        in_specs=[anywhere] * 16,
         out_specs=vmem,
         scratch_shapes=[
             pltpu.VMEM(queries.shape, bf16),
@@ -907,6 +903,7 @@
             pltpu.VMEM((1, rows), jnp.int32),
             pltpu.VMEM(routes.shape[::-1], jnp.int32),
             pltpu.VMEM(routes.shape[::-1], f32),
+            pltpu.SMEM(sinks.shape, f32),
             pltpu.VMEM((1, width), f32),
             pltpu.VMEM((rows, cols), bf16),
             pltpu.VMEM(out_weight.shape, bf16),
@@ -934,7 +931,7 @@
             pltpu.VMEM((4, rows, cols), bf16),
             pltpu.VMEM((5, rows, cols), bf16),
             pltpu.VMEM((rows, cols), f32),
-            dma((len(arguments) - 1,)),
+            dma((11,)),
             dma((4,)),
             dma((3,)),
             dma((4,)),

time: 52.9 us -> 52.1 us (0.985)
  Pallas kernels: 52 us -> 51.2 us
    pallas_call x1, Pallas kernels: 52 us -> 51.2 us  [layer(): pl.pallas_call(functools.partial(fused_kernel, (rows, cols, width, WINDOW...]
where the time goes in v5:
time: 52.1 us; the launch traced here: 51.9 us
  Pallas kernels  51.2 us (98%)
  local copies, waits for them, and re-layouts  0.71 us (1%)
    pallas_call x1, Pallas kernels, layer(): pl.pallas_call(functools.partial(fused_kernel, (rows, cols, width, WINDOW...  51.2 us

profile of v5, /device:TPU:0, one launch (start us, length us, event | category | flops | bytes accessed | tf_op | source)
XLA Modules:
  0.0 51.9 jit_solution(4334811030001095445)
XLA Ops:
  0.0 51.2 %shard_map.154 = bf16[256,512]{1,0:T(8,128)(2,1)S(1)} custom-call(bf16[256,2048]{1,0:T(8,128)(2,1)} %res_hbm.1, bf16[256,256]{1,0:T(8,128)(2,1)} %q_hbm.1, bf16[256,128]{1,0:T(8,128)(2,1)} %k_hbm.1, bf16[256,128]{1,0:T(8,128)(2,1)} %v_hbm.1, s32[1,256]{1,0:T(1,128)} %bitcast.7, s32[2,256]{1,0:T(2,128)} %bitcast.5, f32[2,256]{1,0:T(2,128)} %bitcast.6, ...), custom_call_target="tpu_custom_call" | custom-call | tf_op jit(solution)/shard_map/pallas_call | solution.py:894
  51.2 0.7 %copy.18 = bf16[256,512]{1,0:T(8,128)(2,1)} copy(bf16[256,512]{1,0:T(8,128)(2,1)S(1)} %shard_map.154) | data formatting | bytes 524288

commit v6 on v5

--- a/solution.py
+++ b/solution.py
@@ -220,7 +220,6 @@
     halo_r,
     x_r,
     b_r,
-    c_r,
     u_r,
     m_r,
     a_r,
@@ -408,7 +407,7 @@
         mine = mine + b1r[n, 1].astype(f32)
         for i, p in enumerate(parts_of(n)):
             b2s[p] = mine[i * part_rows : (i + 1) * part_rows].astype(bf16)
-            copy = remote(b2s.at[p], b2r.at[p], c_r.at[p], s, over)
+            copy = remote(b2s.at[p], b2r.at[p], u_r.at[s, 0, p], s, over)
             go(copy)
             second[p] = copy
 
@@ -552,7 +551,7 @@
 
     def back(place, b, p, sp, role=B):
         here = part_span(p)
-        return remote(ret.at[b, here], rin.at[place, here], e_r.at[place, p], sp, t, role)
+        return remote(ret.at[b, here], rin.at[place, here], e_r.at[b, p], sp, t, role)
 
     def give(block, n):
         weighted(block, n, tot.at[index_of(block)], None)
@@ -583,11 +582,15 @@
 
     def gather_in(p):
         here = part_span(p)
-        back(s, s, p, inner).wait_recv()
+        both = rin.at[pl.ds(0, 2), here]
+
+        @pl.when(is_end)
+        def _():
+            back(s, s, p, inner).wait_recv()
 
         @pl.when(is_mid)
         def _():
-            back(4, s, p, outer).wait_recv()
+            remote(both, both, e_r.at[s, p], outer, t).wait_recv()
 
         result[here, :] = (
             acc[here, :] + rin[s, here, :].astype(f32) + rin[4, here, :].astype(f32)
@@ -936,11 +939,10 @@
             dma((3,)),
             dma((4,)),
             dma((blocks, 2)),
-            dma((PARTS,)),
             dma((4, 2, PARTS)),
             dma((4, blocks)),
             dma((5, 2, blocks)),
-            dma((5, PARTS)),
+            dma((4, PARTS)),
         ],
         compiler_params=pltpu.CompilerParams(collective_id=0, has_side_effects=True),
     )(

time: 52.1 us -> 52 us (level)
  no operation moved by 1% of the time
where the time goes in v6:
time: 52 us; the launch traced here: 51.9 us
  Pallas kernels  51.2 us (98%)
  local copies, waits for them, and re-layouts  0.71 us (1%)
    pallas_call x1, Pallas kernels, layer(): pl.pallas_call(functools.partial(fused_kernel, (rows, cols, width, WINDOW...  51.2 us

profile of v6, /device:TPU:0, one launch (start us, length us, event | category | flops | bytes accessed | tf_op | source)
XLA Modules:
  0.0 51.9 jit_solution(15288019278976710366)
XLA Ops:
  0.0 51.2 %shard_map.154 = bf16[256,512]{1,0:T(8,128)(2,1)S(1)} custom-call(bf16[256,2048]{1,0:T(8,128)(2,1)} %res_hbm.1, bf16[256,256]{1,0:T(8,128)(2,1)} %q_hbm.1, bf16[256,128]{1,0:T(8,128)(2,1)} %k_hbm.1, bf16[256,128]{1,0:T(8,128)(2,1)} %v_hbm.1, s32[1,256]{1,0:T(1,128)} %bitcast.7, s32[2,256]{1,0:T(2,128)} %bitcast.5, f32[2,256]{1,0:T(2,128)} %bitcast.6, ...), custom_call_target="tpu_custom_call" | custom-call | tf_op jit(solution)/shard_map/pallas_call | solution.py:897
  51.2 0.7 %copy.18 = bf16[256,512]{1,0:T(8,128)(2,1)} copy(bf16[256,512]{1,0:T(8,128)(2,1)S(1)} %shard_map.154) | data formatting | bytes 524288

commit v7 on v6

--- a/solution.py
+++ b/solution.py
@@ -153,11 +153,11 @@
 OWN = (0, 1)
 E, M, B = 0, 1, 2
 ALONG = {
-    (E, 1): (0, 1, 3),
-    (E, 2): (0,),
+    (E, 1): (0, 1, 2),
+    (E, 2): (1,),
     (E, 3): (1,),
     (M, 0): (0, 1, 2, 3),
-    (M, 2): (0, 3),
+    (M, 2): (1, 2),
     (M, 3): (2, 3),
 }
 
@@ -660,164 +660,164 @@
     enter()
     reduce_in_chip(1)
     reduce_across(1)
-    clear()
     halo()
     attend(0)
+    reduce_in_chip(0)
     loaded(6)
+    hold(1)
     take_weights(M, 0)
-    reduce_in_chip(0)
-    hold(1)
     reduce_across(0)
+    clear()
     publish(2)
     send_own(M, 0, 2, 0)
-    take_weights(M, 2)
     send_own(E, 0, 2, 0)
     send_own(M, 1, 2, 0)
-    hold(0)
+    take_weights(M, 2)
     publish(3)
+    send_own(M, 0, 3, 0)
+    send_own(M, 1, 3, 0)
     loaded(7, 8, 9, 10)
-    send_own(M, 0, 3, 0)
     send_own(E, 0, 3, 0)
-    send_own(M, 1, 3, 0)
     take(M, 0, 2, 0)
     take_weights(M, 3)
     take(M, 2, 2, 0)
+    take(M, 0, 3, 0)
+    hold(0)
     publish(0)
     send_own(E, 0, 0, 0)
-    take(M, 0, 3, 0)
     take(M, 2, 3, 0)
+    publish(1)
+    send_own(E, 0, 1, 0)
     take(M, 0, 0, 0)
-    publish(1)
     take(M, 3, 2, 0)
     take(M, 0, 1, 0)
-    send_own(M, 0, 1, 0)
-    send_own(E, 0, 1, 0)
+    take(M, 3, 3, 0)
+    take_weights(E, 3)
     send_own(M, 0, 0, 0)
+    take(M, 3, 0, 0)
     own_over(3)
+    own_over(2)
     send_own(E, 0, 3, 1)
-    take(M, 3, 3, 0)
-    take(E, 1, 2, 0)
-    take(M, 2, 2, 1)
-    take_weights(E, 3)
-    take(M, 3, 0, 0)
+    take(E, 2, 2, 0)
     own_over(0)
-    own_over(2)
-    send_own(M, 0, 3, 1)
-    take(E, 2, 2, 0)
+    send_own(M, 1, 2, 1)
     send_own(E, 0, 2, 1)
     take(M, 0, 3, 1)
     take(E, 2, 3, 0)
-    send_own(M, 0, 0, 1)
+    take(E, 3, 2, 0)
     take(M, 3, 1, 0)
+    norm_own(1)
+    take(E, 2, 2, 1)
+    take(E, 1, 2, 0)
+    send_own(M, 0, 2, 1)
+    own_over(1)
     take(M, 0, 2, 1)
-    take(E, 3, 2, 0)
-    take(E, 1, 3, 0)
-    take(E, 2, 2, 1)
-    take(M, 2, 1, 0)
-    send_own(M, 1, 3, 1)
-    send_own(E, 0, 0, 1)
     take(E, 3, 3, 0)
     take(E, 2, 3, 1)
-    own_over(1)
-    take(E, 3, 0, 0)
-    send_own(E, 0, 1, 1)
+    send_own(M, 0, 1, 1)
+    take(E, 1, 3, 0)
+    send_own(M, 0, 1, 0)
+    take(M, 2, 0, 0)
+    send_own(E, 0, 0, 1)
     compute((2, 0), 1)
     take(E, 3, 2, 1)
-    norm_own(1)
-    take(E, 1, 2, 1)
+    take(M, 3, 1, 1)
+    send_own(E, 0, 1, 1)
+    take(E, 3, 0, 0)
+    take(M, 2, 3, 1)
+    send_own(M, 1, 1, 0)
     norm_own(0)
     take(E, 3, 3, 1)
-    take(M, 3, 1, 1)
-    take(M, 2, 0, 0)
+    take(M, 2, 2, 1)
+    take_weights(E, 2)
+    compute((3, 2), 1)
+    take(E, 3, 1, 1)
+    take(E, 2, 0, 0)
+    take(M, 3, 2, 1)
+    take(M, 3, 3, 1)
+    take(M, 2, 1, 1)
+    relay_act(E, 2, 1)
+    take(E, 3, 1, 0)
+    take(E, 1, 3, 1)
+    relay_act(M, 0, 1)
+    take(E, 3, 0, 1)
+    take(M, 0, 1, 1)
+    take(M, 3, 0, 1)
+    take(M, 2, 1, 0)
+    take(E, 1, 2, 1)
+    give((2, 0), 1)
+    send_own(M, 1, 1, 1)
+    pass_back(E, 2, 3)
+    compute((3, 3), 0)
+    take(M, 2, 0, 1)
+    pass_back(E, 2, 2)
+    take(E, 2, 1, 1)
+    relay_act(E, 3, 1)
+    take(M, 0, 0, 1)
+    send_own(M, 1, 0, 1)
+    compute((1, 3), 1)
+    take(E, 2, 0, 1)
     take(E, 2, 1, 0)
-    take(M, 2, 3, 1)
-    compute((3, 2), 1)
-    take(M, 0, 1, 1)
-    take(M, 2, 1, 1)
-    relay_act(M, 0, 1)
-    take(M, 3, 0, 1)
-    take_weights(E, 2)
-    take(M, 2, 0, 1)
-    take(E, 3, 1, 0)
+    send_own(M, 1, 0, 0)
+    relay_act(M, 2, 1)
+    give((3, 2), 1)
+    pass_back(E, 3, 2)
+    take_weights(E, 1)
+    compute((2, 0), 0)
+    relay_act(M, 3, 0)
+    pass_back(E, 3, 3)
+    relay_act(E, 3, 0)
     act_shared(0)
-    take(M, 0, 0, 1)
-    take(M, 3, 3, 1)
-    take(E, 1, 3, 1)
-    take(E, 3, 0, 1)
-    relay_act(E, 2, 1)
-    send_own(M, 1, 1, 1)
-    take(E, 3, 1, 1)
-    send_own(M, 1, 0, 0)
-    send_own(M, 1, 1, 0)
-    give((2, 0), 1)
-    pass_back(E, 2, 3)
-    take_weights(E, 1)
-    compute((3, 3), 0)
-    take(M, 3, 2, 1)
-    pass_back(E, 2, 2)
-    take(E, 2, 0, 0)
-    take(E, 2, 1, 1)
-    take(E, 2, 0, 1)
-    send_own(M, 1, 0, 1)
-    relay_act(E, 3, 1)
-    relay_act(M, 2, 1)
-    compute((1, 3), 1)
-    give((3, 2), 1)
-    pass_back(E, 3, 3)
-    pass_back(E, 3, 2)
-    compute((2, 0), 0)
+    take(E, 1, 1, 0)
+    relay_act(M, 3, 1)
+    take(E, 1, 0, 1)
+    pass_back(M, 2, 3)
+    give((3, 3), 0)
+    pass_back(E, 3, 1)
+    take(E, 1, 1, 1)
+    pass_back(E, 3, 0)
+    relay_act(E, 1, 1)
     take(E, 1, 0, 0)
-    relay_act(E, 3, 0)
-    pass_back(M, 2, 3)
-    act_shared(1)
-    relay_act(M, 3, 0)
-    relay_act(B, 1, 0)
-    give((3, 3), 0)
-    pass_back(E, 3, 0)
-    pass_back(E, 3, 1)
-    relay_act(M, 3, 1)
-    take(E, 1, 1, 1)
-    take(E, 1, 1, 0)
-    relay_act(E, 1, 1)
-    take(E, 1, 0, 1)
+    act_own(0)
     give((1, 3), 1)
+    pass_back(M, 3, 2)
+    pass_back(E, 1, 3)
+    compute((1, 2), 0)
     relay_act(M, 0, 0)
+    pass_back(M, 3, 3)
     relay_act(E, 2, 0)
-    pass_back(E, 1, 3)
-    pass_back(M, 3, 3)
-    compute((1, 2), 0)
-    keep_shared(0)
-    pass_back(M, 3, 2)
-    relay_act(B, 1, 1)
-    pass_back(M, 3, 0)
+    act_own(1)
+    pass_back(M, 3, 1)
     give((2, 0), 0)
     pass_back(E, 2, 0)
+    pass_back(M, 0, 2)
+    act_shared(1)
+    relay_act(B, 0, 0)
     pass_back(E, 2, 1)
+    pass_back(M, 3, 0)
+    pass_back(M, 0, 3)
+    relay_act(M, 2, 0)
     pass_back(E, 1, 2)
-    pass_back(M, 0, 3)
-    pass_back(M, 3, 1)
-    act_own(1)
-    relay_act(M, 2, 0)
     relay_act(E, 1, 0)
-    pass_back(M, 0, 2)
     pass_back(M, 2, 2)
-    act_own(0)
+    pass_back(M, 0, 1)
     give((1, 2), 0)
+    relay_act(B, 0, 1)
+    pass_back(M, 2, 0)
     pass_back(M, 0, 0)
+    pass_back(M, 2, 1)
+    pass_back(E, 1, 1)
     pass_back(E, 1, 0)
-    pass_back(M, 2, 0)
-    pass_back(M, 0, 1)
-    relay_act(B, 0, 1)
-    pass_back(E, 1, 1)
-    pass_back(M, 2, 1)
+    relay_act(B, 1, 0)
+    keep_shared(0)
+    keep_own(0)
+    relay_act(B, 1, 1)
     keep_shared(1)
-    relay_act(B, 0, 0)
     keep_own(1)
-    keep_own(0)
+    gather_in(3)
+    gather_in(1)
     gather_in(2)
     gather_in(0)
-    gather_in(3)
-    gather_in(1)
 
     def settle(size, sem):
         for unit in (upd.at[0], upd.at[0, 0], piece(0, 0, 0), wx.at[0]):

time: 52 us -> 51.8 us (level)
  no operation moved by 1% of the time
where the time goes in v7:
time: 51.8 us; the launch traced here: 51.7 us
  Pallas kernels  51 us (98%)
  local copies, waits for them, and re-layouts  0.71 us (1%)
    pallas_call x1, Pallas kernels, layer(): pl.pallas_call(functools.partial(fused_kernel, (rows, cols, width, WINDOW...  51 us

profile of v7, /device:TPU:0, one launch (start us, length us, event | category | flops | bytes accessed | tf_op | source)
XLA Modules:
  0.0 51.7 jit_solution(11359356362881958003)
XLA Ops:
  0.0 51.0 %shard_map.154 = bf16[256,512]{1,0:T(8,128)(2,1)S(1)} custom-call(bf16[256,2048]{1,0:T(8,128)(2,1)} %res_hbm.1, bf16[256,256]{1,0:T(8,128)(2,1)} %q_hbm.1, bf16[256,128]{1,0:T(8,128)(2,1)} %k_hbm.1, bf16[256,128]{1,0:T(8,128)(2,1)} %v_hbm.1, s32[1,256]{1,0:T(1,128)} %bitcast.7, s32[2,256]{1,0:T(2,128)} %bitcast.5, f32[2,256]{1,0:T(2,128)} %bitcast.6, ...), custom_call_target="tpu_custom_call" | custom-call | tf_op jit(solution)/shard_map/pallas_call | solution.py:897
  51.0 0.7 %copy.18 = bf16[256,512]{1,0:T(8,128)(2,1)} copy(bf16[256,512]{1,0:T(8,128)(2,1)S(1)} %shard_map.154) | data formatting | bytes 524288
